TPU v7x, 256 devices: a 4x2x16 block of a 4x16x16 slice. The times are simulated.
256 devices in a mesh: grp: 2 (over y), sp: 16 (over z), fs: 4 (over x), tp: 2 (over core).
Axes of the slice: x: 4, y: 2, z: 16, core: 2. Of those that a mesh axis runs over, the one named last changes fastest.
The devices are a block of a 4x16x16 slice.
Arguments:
- tokens: bfloat16 [8, 2048, 2048], P(('grp', 'fs'), 'sp', 'tp'), parts along dimension 0, may hold values from -120 to 120
- mix_gain: float32 [2048], replicated, may hold values from 0.1 to 1.9
- attn_query: bfloat16 [2048, 1024], P('fs', 'tp'), may hold values from -0.375 to 0.375
- attn_key: bfloat16 [2048, 1024], P('fs', 'tp'), may hold values from -0.125 to 0.125
- attn_value: bfloat16 [2048, 1024], P('fs', 'tp'), may hold values from -0.125 to 0.125
- rec_query: bfloat16 [2048, 1024], P('fs', 'tp'), may hold values from -0.125 to 0.125
- rec_forget: bfloat16 [2048, 1024], P('fs', 'tp'), may hold values from -0.125 to 0.125
- rec_input: bfloat16 [2048, 1024], P('fs', 'tp'), may hold values from -0.125 to 0.125
- break_offset: float32 [8], P('tp'), may hold values from -13.5 to -7
- forget_room: float32 [8, 128], P('tp'), may hold values from 0.00024414062 to 0.05
- out_gain: float32 [128], replicated, may hold values from 0.1 to 1.9
- out_attn: bfloat16 [1024, 2048], P('tp', 'fs'), may hold values from -0.125 to 0.125
- out_rec: bfloat16 [1024, 2048], P('tp', 'fs'), may hold values from -0.125 to 0.125
Outputs:
- mixed: bfloat16 [8, 2048, 2048], P(('grp', 'fs'), ('sp', 'tp')), parts along dimension 0
There are 2 independent parts, one for each index of `grp`. A program takes and returns all parts, laid end to end along the dimension named above; an argument that names none is the same for every part. Nothing has to cross between parts.
All inputs are finite; a program needn't handle non-finite values.
Results may differ from a plain program's by a relative error of at most 0.019.
Values may be sent and summed in bfloat16 or wider, within the bound.
No kernel may reach another device: no remote copies, remote signals or barrier semaphores. Data moves between devices by JAX's collectives and lax.ppermute only.
A program may use at most 64 MiB of HBM per device.

v0:
```python
import math

import jax
import jax.numpy as jnp
from jax import lax
from jax.experimental import pallas as pl
from jax.experimental.pallas import tpu as pltpu
from jax.sharding import PartitionSpec as P


HEAD = 128
NORM_EPS = 1e-06
LOG2E = 1.4426950408889634

f32 = jnp.float32
bf16 = jnp.bfloat16


def mm(a, b):
    return lax.dot_general(a, b, (((1,), (0,)), ((), ())), preferred_element_type=f32)


def mm_t(a, b):
    return lax.dot_general(a, b, (((1,), (1,)), ((), ())), preferred_element_type=f32)


def halves(x):
    top = x.astype(bf16)
    return top, (x - top.astype(f32)).astype(bf16)


def ring(size, step):
    return [(k, (k + step) % size) for k in range(size)]


def shift(x, axis, step):
    return lax.ppermute(x, axis, ring(lax.axis_size(axis), step))


def swap(x):
    return lax.ppermute(x, "tp", [(0, 1), (1, 0)])


def columns_kernel(*refs):
    attn, rec = refs[0:3], refs[3:6]
    out_ref, wide_ref, sems = refs[6:]
    _, local, is_attn = place_of_head()
    at = pl.ds(pl.multiple_of(local * HEAD, HEAD), HEAD)

    def columns(sources):
        copies = [
            pltpu.make_async_copy(sources[k].at[:, at], wide_ref.at[k], sems.at[k]) for k in range(3)
        ]
        for copy in copies:
            copy.start()
        for copy in copies:
            copy.wait()

    @pl.when(is_attn)
    def _():
        columns(attn)

    @pl.when(jnp.logical_not(is_attn))
    def _():
        columns(rec)

    for k in range(3):
        out_ref[k * HEAD : (k + 1) * HEAD, :] = wide_ref[k].T


def pack_kernel(mine_ref, other_ref, out_attn, out_rec, pack_ref, sems):
    rows = out_attn.shape[0]
    copies = [
        pltpu.make_async_copy(out_attn, pack_ref.at[0:rows, :], sems.at[0]),
        pltpu.make_async_copy(out_rec, pack_ref.at[rows : 2 * rows, :], sems.at[1]),
    ]
    for copy in copies:
        copy.start()
    head, _, _ = place_of_head()
    holds = holder_of(head) == lax.axis_index("tp")

    @pl.when(holds)
    def _():
        pack_ref[2 * rows :, :] = mine_ref[...]

    @pl.when(jnp.logical_not(holds))
    def _():
        pack_ref[2 * rows :, :] = other_ref[...]

    for copy in copies:
        copy.wait()


def project_kernel(gain_ref, offset_ref, room_ref, *refs):
    fs = lax.axis_size("fs")
    packs, refs = refs[:fs], refs[fs:]
    query_ref, pair_ref, norm_ref = refs[-3:]
    count = (len(refs) - 3) // 2
    near, far = refs[:count], refs[count : 2 * count]
    rows, half = near[0].shape
    each = packs[0].shape[1]
    x, t = lax.axis_index("fs"), lax.axis_index("tp")
    _, local, _ = place_of_head()
    at_a = pl.ds(pl.multiple_of(t * half, half), half)
    at_b = pl.ds(pl.multiple_of((1 - t) * half, half), half)
    for k in range(count):
        own = slice(k * rows, (k + 1) * rows)
        norm_ref[own, at_a] = near[k][...]
        norm_ref[own, at_b] = far[k][...]
    gain = gain_ref[...]

    def normalize(k, _):
        own = pl.ds(pl.multiple_of(k * rows, rows), rows)
        value = norm_ref[own, :].astype(f32)
        total = jnp.sum(value * value, axis=1, keepdims=True)
        factor = lax.rsqrt(total * (1.0 / (2 * half)) + NORM_EPS)
        norm_ref[own, :] = (value * factor * gain).astype(bf16)
        return 0

    lax.fori_loop(0, count, normalize, 0, unroll=2)
    group = 4 * rows

    def multiply(k, _):
        own = pl.ds(pl.multiple_of(k * group, group), group)
        product = 0.0
        for step in range(fs):
            at = pl.ds(pl.multiple_of((x + step) % fs * each, each), each)
            product += mm_t(norm_ref[own, at], packs[step][packs[step].shape[0] - 3 * HEAD :, :])
        product = product.astype(bf16)
        query_ref[own, :] = product[:, :HEAD]
        pair_ref[own, :] = product[:, HEAD:]
        return 0

    lax.fori_loop(0, count * rows // group, multiply, 0)
    offset = jnp.full((1, HEAD), offset_ref[local], f32)
    rest = jnp.concatenate([room_ref[pl.ds(local, 1), :], offset], 1)
    parts = []
    for _ in range(3):
        parts.append(rest.astype(bf16).astype(f32))
        rest = rest - parts[-1]
    extra = pair_ref.shape[0] - count * rows
    pad = jnp.zeros((extra - 3, 2 * HEAD), f32)
    pair_ref[count * rows :, :] = jnp.concatenate(parts + [pad], 0).astype(bf16)


def stick_body(half, offset, q_ref, kv_ref, sums_ref, out_ref, acc_ref, carry_ref, rows, blocks):
    tile = 4
    span = 2 * rows
    factor = LOG2E / math.sqrt(HEAD)
    offset = jnp.concatenate([offset * LOG2E] * tile, 1)
    strict = (
        lax.broadcasted_iota(jnp.int32, (rows, span), 1)
        < lax.broadcasted_iota(jnp.int32, (rows, span), 0) + half * rows
    )

    def keys_of(group):
        return pl.ds(pl.multiple_of(group * (tile * span), tile * span), tile * span)

    def attend(queries, group, carry, diagonal):
        keys = keys_of(group)
        z = mm_t(queries, kv_ref[keys, 0:HEAD]) * factor + offset
        tail = jnp.log(1.0 + jnp.exp2(-jnp.abs(z))) * LOG2E
        drop = jnp.maximum(z, 0.0) + tail
        take = jnp.minimum(z, 0.0) - tail
        parts = [None] * tile
        for n in reversed(range(tile)):
            across = slice(n * span, (n + 1) * span)
            skip = n * rows if diagonal else 0
            this = drop[skip:, across]
            if diagonal:
                first = jnp.where(strict, this[:rows], 0.0)
                this = jnp.concatenate([first, this[rows:]], 0) if n < tile - 1 else first
            both = mm(jnp.concatenate(halves(this), 1), sums_ref[...])
            stick = jnp.exp2(take[skip:, across] - both[:, :span] - carry[skip:])
            total = both[:, span:]
            if diagonal:
                first = jnp.where(strict, stick[:rows], 0.0)
                stick = jnp.concatenate([first, stick[rows:]], 0) if n < tile - 1 else first
            stick = stick.astype(bf16)
            if skip:
                stick = jnp.concatenate([jnp.zeros((skip, span), bf16), stick], 0)
                total = jnp.concatenate([jnp.zeros((skip, span), f32), total], 0)
            parts[n] = stick
            carry = carry + total
        return mm(jnp.concatenate(parts, 1), kv_ref[keys, HEAD:]), carry

    def query_tile(index, _):
        own = pl.ds(pl.multiple_of(index * (tile * rows), tile * rows), tile * rows)
        start = jnp.zeros((tile * rows, span), f32)
        acc_ref[...], carry_ref[...] = attend(q_ref[own, :], index, start, True)

        def earlier(step, _):
            out, carry = attend(q_ref[own, :], index - 1 - step, carry_ref[...], False)
            acc_ref[...] += out
            carry_ref[...] = carry
            return 0

        lax.fori_loop(0, index, earlier, 0)
        for n in range(tile):
            out_ref[index * tile + n] = acc_ref[n * rows : (n + 1) * rows, :].astype(bf16)
        return 0

    lax.fori_loop(0, blocks // tile, query_tile, 0)


def recur_body(half, room, gain, q_ref, kv_ref, tri, out_ref, cum_ref, rows, blocks):
    span = 2 * rows
    at_once = 2
    causal = (
        lax.broadcasted_iota(jnp.int32, (rows, span), 1)
        <= lax.broadcasted_iota(jnp.int32, (rows, span), 0) + half * rows
    )
    place = pl.multiple_of(half * rows, rows)

    def one_block(block, slot, state):
        keys = pl.ds(pl.multiple_of(block * span, span), span)
        gate = kv_ref[keys, 0:HEAD].astype(f32)
        values = kv_ref[keys, HEAD:]
        key_in = room / (1.0 + jnp.exp(gate))
        log_forget = jnp.log(1.0 - key_in)
        cum = mm(tri, jnp.concatenate(halves(log_forget), 0))
        last = cum[span - 1 : span, :]
        cum_ref[slot] = cum
        own_cum = cum_ref[slot, pl.ds(place, rows), :]
        queries = q_ref[pl.ds(pl.multiple_of(block * rows, rows), rows), :].astype(f32)
        q_dec = (queries * jnp.exp(own_cum)).astype(bf16)
        k_inv = (key_in * jnp.exp(-cum)).astype(bf16)
        k_end = (key_in * jnp.exp(last - cum)).astype(bf16)
        scores = jnp.where(causal, mm_t(q_dec, k_inv), 0.0).astype(bf16)
        raw = mm(scores, values) + mm_t(q_dec, state.astype(bf16))
        fresh = lax.dot_general(values, k_end, (((0,), (0,)), ((), ())), preferred_element_type=f32)
        scale = lax.rsqrt(jnp.mean(raw * raw, axis=1, keepdims=True) + NORM_EPS)
        out_ref[block] = (raw * scale * gain).astype(bf16)
        return state * jnp.exp(last) + fresh

    def some_blocks(step, state):
        for slot in range(at_once):
            state = one_block(step * at_once + slot, slot, state)
        return state

    lax.fori_loop(0, blocks // at_once, some_blocks, jnp.zeros((HEAD, HEAD), f32))


def mixer_kernel(gain_ref, query_ref, mine_ref, other_ref, *refs):
    out_ref, q_ref, kv_ref, acc_ref, carry_ref, cum_ref, sums_ref = refs
    blocks, rows, _ = out_ref.shape
    span = 2 * rows
    place, half = lax.axis_index("sp"), lax.axis_index("tp")
    head, _, is_attn = place_of_head()
    for k in range(blocks):
        block = (place + k) % blocks
        own = slice(k * rows, (k + 1) * rows)
        q_ref[pl.ds(pl.multiple_of(block * rows, rows), rows), :] = query_ref[own, :]
        at = pl.multiple_of((2 * block + half) * rows, rows)
        kv_ref[pl.ds(at, rows), :] = mine_ref[own, :]
        at = pl.multiple_of((2 * block + 1 - half) * rows, rows)
        kv_ref[pl.ds(at, rows), :] = other_ref[own, :]
    used = blocks * rows
    holds = holder_of(head) == half
    parts = jnp.where(
        holds, mine_ref[used : used + 8, :].astype(f32), other_ref[used : used + 8, :].astype(f32)
    )
    params = parts[0:1, :] + parts[1:2, :] + parts[2:3, :]
    room, offset = params[:, :HEAD], params[:, HEAD:]
    down = lax.broadcasted_iota(jnp.int32, (span, span), 0)
    across = lax.broadcasted_iota(jnp.int32, (span, span), 1)

    @pl.when(is_attn)
    def _():
        later = jnp.where(down > across, 1.0, 0.0).astype(bf16)
        for k in range(2):
            sums_ref[k * span : (k + 1) * span, 0:span] = later
            sums_ref[k * span : (k + 1) * span, span:] = jnp.ones((span, span), bf16)
        stick_body(half, offset, q_ref, kv_ref, sums_ref, out_ref, acc_ref, carry_ref, rows, blocks)

    @pl.when(jnp.logical_not(is_attn))
    def _():
        upto = jnp.where(down >= across, 1.0, 0.0).astype(bf16)
        tri = jnp.concatenate([upto, upto], 1)
        recur_body(half, room, gain_ref[...], q_ref, kv_ref, tri, out_ref, cum_ref, rows, blocks)


def output_kernel(heads_ref, *refs):
    out_ref = refs[-1]
    fs = lax.axis_size("fs")
    x, half = lax.axis_index("fs"), lax.axis_index("tp")
    pieces = refs[:fs], refs[fs : 2 * fs]
    width = pieces[0][0].shape[1]
    depth = heads_ref.shape[0] // 2 * HEAD
    heads = heads_ref.shape[0] // 2
    each = heads // 2
    sides = []
    for core in range(2):
        first = each * (half if core == 0 else 1 - half)
        sides.append(
            jnp.concatenate(
                [heads_ref[kind * heads + first + k] for kind in range(2) for k in range(each)], 1
            )
        )
    for step in range(fs):
        total = sum(mm(sides[core], pieces[core][step][0:depth, :]) for core in range(2))
        at = pl.multiple_of((x + step) % fs * width, width)
        out_ref[:, pl.ds(at, width)] = total.astype(bf16)


PARAM_ROWS = 16

MIB = 1 << 20


def limit(mib):
    return pltpu.CompilerParams(vmem_limit_bytes=mib * MIB)


def resident(arrays):
    return [pltpu.with_memory_space_constraint(a, pltpu.VMEM) for a in arrays]


def left_out(arrays):
    return [pltpu.with_memory_space_constraint(a, pltpu.HBM) for a in arrays]


whole = pl.BlockSpec(memory_space=pltpu.VMEM)
scalar = pl.BlockSpec(memory_space=pltpu.SMEM)
outside = pl.BlockSpec(memory_space=pltpu.HBM)


def place_of_head():
    heads = lax.axis_size("sp") // 2
    place = lax.axis_index("sp")
    head = place % heads
    return head, head % (heads // lax.axis_size("tp")), place < heads


def holder_of(head):
    return head // (lax.axis_size("sp") // 2 // lax.axis_size("tp"))


def body(
    tokens,
    mix_gain,
    attn_query,
    attn_key,
    attn_value,
    rec_query,
    rec_forget,
    rec_input,
    break_offset,
    forget_room,
    out_gain,
    out_attn,
    out_rec,
):
    sp, fs, tp = (lax.axis_size(a) for a in ("sp", "fs", "tp"))
    t = lax.axis_index("tp")
    _, _, _ = place_of_head()

    rows = tokens.shape[1] // tp
    half_width = tokens.shape[2]
    own = tokens[0]
    near = lax.dynamic_slice_in_dim(own, t * rows, rows, 0)
    far = swap(lax.dynamic_slice_in_dim(own, (1 - t) * rows, rows, 0))

    depth, wide = out_attn.shape
    shape = jax.ShapeDtypeStruct((3 * HEAD, attn_query.shape[0]), bf16)
    pick = pl.pallas_call(
        columns_kernel,
        out_shape=shape,
        in_specs=[outside] * 6,
        out_specs=whole,
        scratch_shapes=[
            pltpu.VMEM((3, attn_query.shape[0], HEAD), bf16),
            pltpu.SemaphoreType.DMA((3,)),
        ],
        compiler_params=limit(6),
        name="columns",
    )
    columns = pick(*left_out([attn_query, attn_key, attn_value, rec_query, rec_forget, rec_input]))
    columns_other = swap(columns)
    pack = pl.pallas_call(
        pack_kernel,
        out_shape=jax.ShapeDtypeStruct((2 * depth + shape.shape[0], wide), bf16),
        in_specs=[whole, whole, outside, outside],
        out_specs=whole,
        scratch_shapes=[pltpu.SemaphoreType.DMA((2,))],
        compiler_params=limit(8),
        name="pack",
    )
    pack = pack(*resident([columns, columns_other]), *left_out([out_attn, out_rec]))
    from_prev, from_next = shift(pack, "fs", 1), shift(pack, "fs", -1)
    far_columns = from_prev[2 * depth :]
    far_columns = shift(far_columns, "fs", 1)
    from_far = shift(from_prev, "fs", 1)
    mine = [pack, from_next, from_far, from_prev]
    other_own, other_next, other_prev = swap(pack), swap(from_next), swap(from_prev)
    other_far = swap(from_far)
    other = [other_own, other_next, other_far, other_prev]

    last = sp // 2
    near_blocks, far_blocks = {0: near}, {0: far}
    ahead = [near, far]
    behind = [near, far]
    for hop in range(1, last + 1):
        for k, store in enumerate((near_blocks, far_blocks)):
            if hop < last or k == 0:
                ahead[k] = shift(ahead[k], "sp", 1)
                store[sp - hop] = ahead[k]
            if hop < last or k == 1:
                behind[k] = shift(behind[k], "sp", -1)
                store[hop] = behind[k]

    query, pair = pl.pallas_call(
        project_kernel,
        out_shape=(
            jax.ShapeDtypeStruct((sp * rows, HEAD), bf16),
            jax.ShapeDtypeStruct((sp * rows + PARAM_ROWS, 2 * HEAD), bf16),
        ),
        in_specs=[whole, scalar] + [whole] * (1 + fs + 2 * sp),
        out_specs=(whole, whole),
        scratch_shapes=[pltpu.VMEM((sp * rows, 2 * half_width), bf16)],
        compiler_params=limit(12),
        name="project",
    )(
        mix_gain[None, :],
        break_offset,
        forget_room,
        *resident([pack, from_next, far_columns, from_prev]),
        *resident([near_blocks[s] for s in range(sp)]),
        *resident([far_blocks[s] for s in range(sp)]),
    )
    pair_other = swap(pair)

    span = rows * tp
    mixed_heads = pl.pallas_call(
        mixer_kernel,
        out_shape=jax.ShapeDtypeStruct((sp, rows, HEAD), bf16),
        in_specs=[whole] * 4,
        out_specs=whole,
        scratch_shapes=[
            pltpu.VMEM((sp * rows, HEAD), bf16),
            pltpu.VMEM((sp * span, 2 * HEAD), bf16),
            pltpu.VMEM((4 * rows, HEAD), f32),
            pltpu.VMEM((4 * rows, HEAD), f32),
            pltpu.VMEM((2, span, HEAD), f32),
            pltpu.VMEM((2 * span, 2 * span), bf16),
        ],
        compiler_params=limit(12),
        name="mixer",
    )(out_gain[None, :], *resident([query, pair, pair_other]))

    arrived = lax.all_to_all(mixed_heads, "sp", split_axis=0, concat_axis=0, tiled=True)
    mixed = pl.pallas_call(
        output_kernel,
        out_shape=jax.ShapeDtypeStruct((rows, fs * out_attn.shape[1]), bf16),
        in_specs=[whole] * (1 + 2 * fs),
        out_specs=whole,
        compiler_params=limit(16),
        name="output",
    )(*resident([arrived, *mine, *other]))
    return mixed[None]


def solution(mesh):
    placed = (
        P(("grp", "fs"), "sp", "tp"),
        P(),
        P("fs", "tp"),
        P("fs", "tp"),
        P("fs", "tp"),
        P("fs", "tp"),
        P("fs", "tp"),
        P("fs", "tp"),
        P("tp"),
        P("tp", None),
        P(),
        P("tp", "fs"),
        P("tp", "fs"),
    )
    return jax.shard_map(
        body,
        mesh=mesh,
        in_specs=placed,
        out_specs=P(("grp", "fs"), ("sp", "tp"), None),
        check_vma=False,
    )
```

profile of v0, /device:TPU:46, one launch (start us, length us, event | category | flops | bytes accessed | tf_op | source)
XLA Modules:
  0.0 171.7 jit_solution(14411004651031651320)
XLA Ops:
  4.8 2.8 %collective-permute-start.11 = (bf16[64,1024]{1,0:T(8,128)(2,1)S(1)}, bf16[64,1024]{1,0:T(8,128)(2,1)S(1)}, u32[]{:S(2)}, u32[]{:S(2)}) collective-permute-start(bf16[64,1024]{1,0:T(8,128)(2,1)S(1)} %get-tuple-element.10.refs_4_), channel_id=1, source_target_pairs={{0,8},{8,16},{16,24},{24,32},{32,40},{40,48},{48,56},{56,64},{64,7... | collective-permute-start | bytes 393224 | tf_op jit(solution)/shard_map/ppermute | solution.py:37
  7.6 19.7 %collective-permute-start.4 = (bf16[64,1024]{1,0:T(8,128)(2,1)S(1)}, bf16[64,1024]{1,0:T(8,128)(2,1)S(1)}, u32[]{:S(2)}, u32[]{:S(2)}) collective-permute-start(bf16[64,1024]{1,0:T(8,128)(2,1)S(1)} %get-tuple-element.10.refs_4_), channel_id=1, source_target_pairs={{0,120},{8,0},{16,8},{24,16},{32,24},{40,32},{48,40},{56,48},{64,5... | collective-permute-start | bytes 393224 | tf_op jit(solution)/shard_map/ppermute | solution.py:37
  27.3 1.9 %collective-permute-start.20 = (bf16[64,1024]{1,0:T(8,128)(2,1)S(1)}, bf16[64,1024]{1,0:T(8,128)(2,1)S(1)}, u32[]{:S(2)}, u32[]{:S(2)}) collective-permute-start(bf16[64,1024]{1,0:T(8,128)(2,1)S(1)} %collective-permute-done.19.refs_20_), channel_id=1, source_target_pairs={{0,120},{8,0},{16,8},{24,16},{32,24},{40,32},{48,40},{56,48},{64,5... | collective-permute-start | bytes 393224 | tf_op jit(solution)/shard_map/ppermute | solution.py:37
  29.2 2.0 %collective-permute-start.1 = (bf16[1408,512]{1,0:T(8,128)(2,1)S(1)}, bf16[1408,512]{1,0:T(8,128)(2,1)}, u32[]{:S(2)}, u32[]{:S(2)}) collective-permute-start(bf16[1408,512]{1,0:T(8,128)(2,1)S(1)} %pack.1.refs_0_), channel_id=1, source_target_pairs={{0,6},{2,0},{4,2},{6,4},{1,7},{3,1},{5,3},{7,5},{8,14},{10,8},{12,... | collective-permute-start | bytes 4325384 | tf_op jit(solution)/shard_map/ppermute | solution.py:37
  31.2 6.9 %collective-permute-done.2.refs_3_ = bf16[1408,512]{1,0:T(8,128)(2,1)S(1)} collective-permute-done((bf16[1408,512]{1,0:T(8,128)(2,1)S(1)}, bf16[1408,512]{1,0:T(8,128)(2,1)S(1)}, u32[]{:S(2)}, u32[]{:S(2)}) %collective-permute-start.2) | collective-permute-done | bytes 1441824 | tf_op jit(solution)/shard_map/ppermute | solution.py:37
  39.6 2.8 %collective-permute-start.12 = (bf16[64,1024]{1,0:T(8,128)(2,1)S(1)}, bf16[64,1024]{1,0:T(8,128)(2,1)S(1)}, u32[]{:S(2)}, u32[]{:S(2)}) collective-permute-start(bf16[64,1024]{1,0:T(8,128)(2,1)S(1)} %collective-permute-done.11.refs_19_), channel_id=1, source_target_pairs={{0,8},{8,16},{16,24},{24,32},{32,40},{40,48},{48,56},{56,64},{64,7... | collective-permute-start | bytes 393224 | tf_op jit(solution)/shard_map/ppermute | solution.py:37
  42.4 2.8 %collective-permute-start.28 = (bf16[64,1024]{1,0:T(8,128)(2,1)S(1)}, bf16[64,1024]{1,0:T(8,128)(2,1)S(1)}, u32[]{:S(2)}, u32[]{:S(2)}) collective-permute-start(bf16[64,1024]{1,0:T(8,128)(2,1)S(1)} %collective-permute-done.19.refs_20_), channel_id=1, source_target_pairs={{0,8},{8,16},{16,24},{24,32},{32,40},{40,48},{48,56},{56,64},{64,7... | collective-permute-start | bytes 393224 | tf_op jit(solution)/shard_map/ppermute | solution.py:37
  45.2 17.1 %collective-permute-start.5 = (bf16[64,1024]{1,0:T(8,128)(2,1)S(1)}, bf16[64,1024]{1,0:T(8,128)(2,1)S(1)}, u32[]{:S(2)}, u32[]{:S(2)}) collective-permute-start(bf16[64,1024]{1,0:T(8,128)(2,1)S(1)} %collective-permute-done.4.refs_5_), channel_id=1, source_target_pairs={{0,120},{8,0},{16,8},{24,16},{32,24},{40,32},{48,40},{56,48},{64,5... | collective-permute-start | bytes 393224 | tf_op jit(solution)/shard_map/ppermute | solution.py:37
  62.2 4.0 %collective-permute-done.12.refs_18_ = bf16[64,1024]{1,0:T(8,128)(2,1)S(1)} collective-permute-done((bf16[64,1024]{1,0:T(8,128)(2,1)S(1)}, bf16[64,1024]{1,0:T(8,128)(2,1)S(1)}, u32[]{:S(2)}, u32[]{:S(2)}) %collective-permute-start.12) | collective-permute-done | bytes 131104 | tf_op jit(solution)/shard_map/ppermute | solution.py:37
  66.3 1.7 %collective-permute-start.21 = (bf16[64,1024]{1,0:T(8,128)(2,1)S(1)}, bf16[64,1024]{1,0:T(8,128)(2,1)S(1)}, u32[]{:S(2)}, u32[]{:S(2)}) collective-permute-start(bf16[64,1024]{1,0:T(8,128)(2,1)S(1)} %collective-permute-done.20.refs_21_), channel_id=1, source_target_pairs={{0,120},{8,0},{16,8},{24,16},{32,24},{40,32},{48,40},{56,48},{64,5... | collective-permute-start | bytes 393224 | tf_op jit(solution)/shard_map/ppermute | solution.py:37
  68.4 3.6 %collective-permute-done.21.refs_22_ = bf16[64,1024]{1,0:T(8,128)(2,1)S(1)} collective-permute-done((bf16[64,1024]{1,0:T(8,128)(2,1)S(1)}, bf16[64,1024]{1,0:T(8,128)(2,1)S(1)}, u32[]{:S(2)}, u32[]{:S(2)}) %collective-permute-start.21) | collective-permute-done | bytes 131104 | tf_op jit(solution)/shard_map/ppermute | solution.py:37
  72.0 2.2 %collective-permute-start.6 = (bf16[64,1024]{1,0:T(8,128)(2,1)S(1)}, bf16[64,1024]{1,0:T(8,128)(2,1)S(1)}, u32[]{:S(2)}, u32[]{:S(2)}) collective-permute-start(bf16[64,1024]{1,0:T(8,128)(2,1)S(1)} %collective-permute-done.5.refs_6_), channel_id=1, source_target_pairs={{0,120},{8,0},{16,8},{24,16},{32,24},{40,32},{48,40},{56,48},{64,5... | collective-permute-start | bytes 393224 | tf_op jit(solution)/shard_map/ppermute | solution.py:37
  76.9 3.6 %collective-permute-done.22.refs_23_ = bf16[64,1024]{1,0:T(8,128)(2,1)S(1)} collective-permute-done((bf16[64,1024]{1,0:T(8,128)(2,1)S(1)}, bf16[64,1024]{1,0:T(8,128)(2,1)S(1)}, u32[]{:S(2)}, u32[]{:S(2)}) %collective-permute-start.22) | collective-permute-done | bytes 131104 | tf_op jit(solution)/shard_map/ppermute | solution.py:37
  80.6 2.0 %collective-permute-start.7 = (bf16[64,1024]{1,0:T(8,128)(2,1)S(1)}, bf16[64,1024]{1,0:T(8,128)(2,1)S(1)}, u32[]{:S(2)}, u32[]{:S(2)}) collective-permute-start(bf16[64,1024]{1,0:T(8,128)(2,1)S(1)} %collective-permute-done.6.refs_7_), channel_id=1, source_target_pairs={{0,120},{8,0},{16,8},{24,16},{32,24},{40,32},{48,40},{56,48},{64,5... | collective-permute-start | bytes 393224 | tf_op jit(solution)/shard_map/ppermute | solution.py:37
  86.1 2.9 %collective-permute-done.23.refs_24_ = bf16[64,1024]{1,0:T(8,128)(2,1)S(1)} collective-permute-done((bf16[64,1024]{1,0:T(8,128)(2,1)S(1)}, bf16[64,1024]{1,0:T(8,128)(2,1)S(1)}, u32[]{:S(2)}, u32[]{:S(2)}) %collective-permute-start.23) | collective-permute-done | bytes 131104 | tf_op jit(solution)/shard_map/ppermute | solution.py:37
  89.0 3.2 %collective-permute-start.8 = (bf16[64,1024]{1,0:T(8,128)(2,1)S(1)}, bf16[64,1024]{1,0:T(8,128)(2,1)S(1)}, u32[]{:S(2)}, u32[]{:S(2)}) collective-permute-start(bf16[64,1024]{1,0:T(8,128)(2,1)S(1)} %collective-permute-done.7.refs_8_), channel_id=1, source_target_pairs={{0,120},{8,0},{16,8},{24,16},{32,24},{40,32},{48,40},{56,48},{64,5... | collective-permute-start | bytes 393224 | tf_op jit(solution)/shard_map/ppermute | solution.py:37
  94.2 1.9 %collective-permute-done.8.refs_9_ = bf16[64,1024]{1,0:T(8,128)(2,1)S(1)} collective-permute-done((bf16[64,1024]{1,0:T(8,128)(2,1)S(1)}, bf16[64,1024]{1,0:T(8,128)(2,1)S(1)}, u32[]{:S(2)}, u32[]{:S(2)}) %collective-permute-start.8) | collective-permute-done | bytes 131104 | tf_op jit(solution)/shard_map/ppermute | solution.py:37
  96.1 2.5 %collective-permute-done.24.refs_25_ = bf16[64,1024]{1,0:T(8,128)(2,1)S(1)} collective-permute-done((bf16[64,1024]{1,0:T(8,128)(2,1)S(1)}, bf16[64,1024]{1,0:T(8,128)(2,1)S(1)}, u32[]{:S(2)}, u32[]{:S(2)}) %collective-permute-start.24) | collective-permute-done | bytes 131104 | tf_op jit(solution)/shard_map/ppermute | solution.py:37
  98.5 3.7 %collective-permute-start.9 = (bf16[64,1024]{1,0:T(8,128)(2,1)S(1)}, bf16[64,1024]{1,0:T(8,128)(2,1)S(1)}, u32[]{:S(2)}, u32[]{:S(2)}) collective-permute-start(bf16[64,1024]{1,0:T(8,128)(2,1)S(1)} %collective-permute-done.8.refs_9_), channel_id=1, source_target_pairs={{0,120},{8,0},{16,8},{24,16},{32,24},{40,32},{48,40},{56,48},{64,5... | collective-permute-start | bytes 393224 | tf_op jit(solution)/shard_map/ppermute | solution.py:37
  104.3 1.9 %collective-permute-done.9.refs_10_ = bf16[64,1024]{1,0:T(8,128)(2,1)S(1)} collective-permute-done((bf16[64,1024]{1,0:T(8,128)(2,1)S(1)}, bf16[64,1024]{1,0:T(8,128)(2,1)S(1)}, u32[]{:S(2)}, u32[]{:S(2)}) %collective-permute-start.9) | collective-permute-done | bytes 131104 | tf_op jit(solution)/shard_map/ppermute | solution.py:37
  106.1 1.9 %collective-permute-done.25.refs_26_ = bf16[64,1024]{1,0:T(8,128)(2,1)S(1)} collective-permute-done((bf16[64,1024]{1,0:T(8,128)(2,1)S(1)}, bf16[64,1024]{1,0:T(8,128)(2,1)S(1)}, u32[]{:S(2)}, u32[]{:S(2)}) %collective-permute-start.25) | collective-permute-done | bytes 131104 | tf_op jit(solution)/shard_map/ppermute | solution.py:37
  108.1 3.4 %collective-permute-start.10 = (bf16[64,1024]{1,0:T(8,128)(2,1)S(1)}, bf16[64,1024]{1,0:T(8,128)(2,1)S(1)}, u32[]{:S(2)}, u32[]{:S(2)}) collective-permute-start(bf16[64,1024]{1,0:T(8,128)(2,1)S(1)} %collective-permute-done.9.refs_10_), channel_id=1, source_target_pairs={{0,120},{8,0},{16,8},{24,16},{32,24},{40,32},{48,40},{56,48},{64,5... | collective-permute-start | bytes 393224 | tf_op jit(solution)/shard_map/ppermute | solution.py:37
  111.6 2.4 %collective-permute-done.33.refs_30_ = bf16[64,1024]{1,0:T(8,128)(2,1)S(1)} collective-permute-done((bf16[64,1024]{1,0:T(8,128)(2,1)S(1)}, bf16[64,1024]{1,0:T(8,128)(2,1)S(1)}, u32[]{:S(2)}, u32[]{:S(2)}) %collective-permute-start.33) | collective-permute-done | bytes 131104 | tf_op jit(solution)/shard_map/ppermute | solution.py:37
  116.1 2.9 %collective-permute-done.26.refs_27_ = bf16[64,1024]{1,0:T(8,128)(2,1)S(1)} collective-permute-done((bf16[64,1024]{1,0:T(8,128)(2,1)S(1)}, bf16[64,1024]{1,0:T(8,128)(2,1)S(1)}, u32[]{:S(2)}, u32[]{:S(2)}) %collective-permute-start.26) | collective-permute-done | bytes 131104 | tf_op jit(solution)/shard_map/ppermute | solution.py:37
  119.0 2.9 %collective-permute-done.18.refs_12_ = bf16[64,1024]{1,0:T(8,128)(2,1)S(1)} collective-permute-done((bf16[64,1024]{1,0:T(8,128)(2,1)S(1)}, bf16[64,1024]{1,0:T(8,128)(2,1)S(1)}, u32[]{:S(2)}, u32[]{:S(2)}) %collective-permute-start.18) | collective-permute-done | bytes 131104 | tf_op jit(solution)/shard_map/ppermute | solution.py:37
  123.2 2.1 %collective-permute-done.34.refs_29_ = bf16[64,1024]{1,0:T(8,128)(2,1)S(1)} collective-permute-done((bf16[64,1024]{1,0:T(8,128)(2,1)S(1)}, bf16[64,1024]{1,0:T(8,128)(2,1)S(1)}, u32[]{:S(2)}, u32[]{:S(2)}) %collective-permute-start.34) | collective-permute-done | bytes 131104 | tf_op jit(solution)/shard_map/ppermute | solution.py:37
  125.2 1.7 %collective-permute-done.27.refs_28_ = bf16[64,1024]{1,0:T(8,128)(2,1)S(1)} collective-permute-done((bf16[64,1024]{1,0:T(8,128)(2,1)S(1)}, bf16[64,1024]{1,0:T(8,128)(2,1)S(1)}, u32[]{:S(2)}, u32[]{:S(2)}) %collective-permute-start.27) | collective-permute-done | bytes 131104 | tf_op jit(solution)/shard_map/ppermute | solution.py:37
  127.0 7.1 %project.1 = (bf16[1024,128]{1,0:T(8,128)(2,1)S(1)}, bf16[1040,256]{1,0:T(8,128)(2,1)S(1)}) custom-call(f32[1,2048]{1,0:T(1,128)S(1)} %bitcast.7, f32[4]{0:T(128)S(1)} %copy-done.2, f32[4,128]{1,0:T(4,128)S(1)} %copy-done.1, bf16[1408,512]{1,0:T(8,128)(2,1)S(1)} %pack.1.refs_0_, bf16[1408,512]{1,0:T(8,128)(2,1)} %collective-permute-done.1.refs_1_, ...), custom_call_target="tpu_custom_call" | custom-call | tf_op jit(solution)/shard_map/project/pallas_call | solution.py:412
  136.2 7.6 %mixer.1 = bf16[16,64,128]{2,1,0:T(8,128)(2,1)} custom-call(f32[1,128]{1,0:T(1,128)S(1)} %bitcast.8, bf16[1024,128]{1,0:T(8,128)(2,1)S(1)} %get-tuple-element.7.query_ref, bf16[1040,256]{1,0:T(8,128)(2,1)S(1)} %get-tuple-element.8.mine_ref, bf16[1040,256]{1,0:T(8,128)(2,1)S(1)} %collective-permute-done.35.other_ref), custom_call_target="tpu_custom_call" | custom-call | tf_op jit(solution)/shard_map/mixer/pallas_call | solution.py:434
  143.8 4.0 %all-to-all-start = ((bf16[16,64,128]{2,1,0:T(8,128)(2,1)}), bf16[16,64,128]{2,1,0:T(8,128)(2,1)S(1)}, u32[]{:S(2)}, u32[]{:S(2)}) async-start(bf16[16,64,128]{2,1,0:T(8,128)(2,1)} %mixer.1), calls=%async_computation | async-start | bytes 524288 | tf_op jit(solution)/shard_map/all_to_all | solution.py:451
  147.8 18.2 %all-to-all-done.heads_ref = bf16[16,64,128]{2,1,0:T(8,128)(2,1)S(1)} async-done(((bf16[16,64,128]{2,1,0:T(8,128)(2,1)}), bf16[16,64,128]{2,1,0:T(8,128)(2,1)S(1)}, u32[]{:S(2)}, u32[]{:S(2)}) %all-to-all-start) | async-done | bytes 262176 | tf_op jit(solution)/shard_map/all_to_all | solution.py:451
  166.0 5.8 %output.1 = bf16[64,2048]{1,0:T(8,128)(2,1)} custom-call(bf16[16,64,128]{2,1,0:T(8,128)(2,1)S(1)} %all-to-all-done.heads_ref, bf16[1408,512]{1,0:T(8,128)(2,1)S(1)} %pack.1.refs_0_, bf16[1408,512]{1,0:T(8,128)(2,1)} %collective-permute-done.1.refs_1_, bf16[1408,512]{1,0:T(8,128)(2,1)} %collective-permute-done.36.refs_2_, ...), custom_call_target="tpu_custom_call" | custom-call | tf_op jit(solution)/shard_map/output/pallas_call | solution.py:452
  (69 shorter events, 22.4 us)
Async XLA Ops:
  4.3 33.7 %collective-permute-start.2 = (bf16[1408,512]{1,0:T(8,128)(2,1)S(1)}, bf16[1408,512]{1,0:T(8,128)(2,1)S(1)}, u32[]{:S(2)}, u32[]{:S(2)}) collective-permute-start(bf16[1408,512]{1,0:T(8,128)(2,1)S(1)} %pack.1.refs_0_), channel_id=1, source_target_pairs={{0,2},{2,4},{4,6},{6,0},{1,3},{3,5},{5,7},{7,1},{8,10},{10,12},{12... | collective-permute-start | bytes 4325384 | tf_op jit(solution)/shard_map/ppermute | solution.py:37
  4.6 22.8 %collective-permute-start.19 = (bf16[64,1024]{1,0:T(8,128)(2,1)S(1)}, bf16[64,1024]{1,0:T(8,128)(2,1)S(1)}, u32[]{:S(2)}, u32[]{:S(2)}) collective-permute-start(bf16[64,1024]{1,0:T(8,128)(2,1)S(1)} %get-tuple-element.9), channel_id=1, source_target_pairs={{0,1},{1,0},{2,3},{3,2},{4,5},{5,4},{6,7},{7,6},{8,9},{9,8},{10,11... | collective-permute-start | bytes 393224 | tf_op jit(solution)/shard_map/ppermute | solution.py:41
  4.8 34.8 %collective-permute-start.11 = (bf16[64,1024]{1,0:T(8,128)(2,1)S(1)}, bf16[64,1024]{1,0:T(8,128)(2,1)S(1)}, u32[]{:S(2)}, u32[]{:S(2)}) collective-permute-start(bf16[64,1024]{1,0:T(8,128)(2,1)S(1)} %get-tuple-element.10.refs_4_), channel_id=1, source_target_pairs={{0,8},{8,16},{16,24},{24,32},{32,40},{40,48},{48,56},{56,64},{64,7... | collective-permute-start | bytes 393224 | tf_op jit(solution)/shard_map/ppermute | solution.py:37
  7.6 34.8 %collective-permute-start.4 = (bf16[64,1024]{1,0:T(8,128)(2,1)S(1)}, bf16[64,1024]{1,0:T(8,128)(2,1)S(1)}, u32[]{:S(2)}, u32[]{:S(2)}) collective-permute-start(bf16[64,1024]{1,0:T(8,128)(2,1)S(1)} %get-tuple-element.10.refs_4_), channel_id=1, source_target_pairs={{0,120},{8,0},{16,8},{24,16},{32,24},{40,32},{48,40},{56,48},{64,5... | collective-permute-start | bytes 393224 | tf_op jit(solution)/shard_map/ppermute | solution.py:37
  27.3 17.8 %collective-permute-start.20 = (bf16[64,1024]{1,0:T(8,128)(2,1)S(1)}, bf16[64,1024]{1,0:T(8,128)(2,1)S(1)}, u32[]{:S(2)}, u32[]{:S(2)}) collective-permute-start(bf16[64,1024]{1,0:T(8,128)(2,1)S(1)} %collective-permute-done.19.refs_20_), channel_id=1, source_target_pairs={{0,120},{8,0},{16,8},{24,16},{32,24},{40,32},{48,40},{56,48},{64,5... | collective-permute-start | bytes 393224 | tf_op jit(solution)/shard_map/ppermute | solution.py:37
  29.2 97.7 %collective-permute-start.1 = (bf16[1408,512]{1,0:T(8,128)(2,1)S(1)}, bf16[1408,512]{1,0:T(8,128)(2,1)}, u32[]{:S(2)}, u32[]{:S(2)}) collective-permute-start(bf16[1408,512]{1,0:T(8,128)(2,1)S(1)} %pack.1.refs_0_), channel_id=1, source_target_pairs={{0,6},{2,0},{4,2},{6,4},{1,7},{3,1},{5,3},{7,5},{8,14},{10,8},{12,... | collective-permute-start | bytes 4325384 | tf_op jit(solution)/shard_map/ppermute | solution.py:37
  38.1 97.2 %collective-permute-start.36 = (bf16[1408,512]{1,0:T(8,128)(2,1)S(1)}, bf16[1408,512]{1,0:T(8,128)(2,1)}, u32[]{:S(2)}, u32[]{:S(2)}) collective-permute-start(bf16[1408,512]{1,0:T(8,128)(2,1)S(1)} %collective-permute-done.2.refs_3_), channel_id=1, source_target_pairs={{0,2},{2,4},{4,6},{6,0},{1,3},{3,5},{5,7},{7,1},{8,10},{10,12},{12... | collective-permute-start | bytes 4325384 | tf_op jit(solution)/shard_map/ppermute | solution.py:37
  39.6 26.7 %collective-permute-start.12 = (bf16[64,1024]{1,0:T(8,128)(2,1)S(1)}, bf16[64,1024]{1,0:T(8,128)(2,1)S(1)}, u32[]{:S(2)}, u32[]{:S(2)}) collective-permute-start(bf16[64,1024]{1,0:T(8,128)(2,1)S(1)} %collective-permute-done.11.refs_19_), channel_id=1, source_target_pairs={{0,8},{8,16},{16,24},{24,32},{32,40},{40,48},{48,56},{56,64},{64,7... | collective-permute-start | bytes 393224 | tf_op jit(solution)/shard_map/ppermute | solution.py:37
  42.4 25.6 %collective-permute-start.28 = (bf16[64,1024]{1,0:T(8,128)(2,1)S(1)}, bf16[64,1024]{1,0:T(8,128)(2,1)S(1)}, u32[]{:S(2)}, u32[]{:S(2)}) collective-permute-start(bf16[64,1024]{1,0:T(8,128)(2,1)S(1)} %collective-permute-done.19.refs_20_), channel_id=1, source_target_pairs={{0,8},{8,16},{16,24},{24,32},{32,40},{40,48},{48,56},{56,64},{64,7... | collective-permute-start | bytes 393224 | tf_op jit(solution)/shard_map/ppermute | solution.py:37
  45.2 23.1 %collective-permute-start.5 = (bf16[64,1024]{1,0:T(8,128)(2,1)S(1)}, bf16[64,1024]{1,0:T(8,128)(2,1)S(1)}, u32[]{:S(2)}, u32[]{:S(2)}) collective-permute-start(bf16[64,1024]{1,0:T(8,128)(2,1)S(1)} %collective-permute-done.4.refs_5_), channel_id=1, source_target_pairs={{0,120},{8,0},{16,8},{24,16},{32,24},{40,32},{48,40},{56,48},{64,5... | collective-permute-start | bytes 393224 | tf_op jit(solution)/shard_map/ppermute | solution.py:37
  68.0 6.3 %collective-permute-start.13 = (bf16[64,1024]{1,0:T(8,128)(2,1)S(1)}, bf16[64,1024]{1,0:T(8,128)(2,1)S(1)}, u32[]{:S(2)}, u32[]{:S(2)}) collective-permute-start(bf16[64,1024]{1,0:T(8,128)(2,1)S(1)} %collective-permute-done.12.refs_18_), channel_id=1, source_target_pairs={{0,8},{8,16},{16,24},{24,32},{32,40},{40,48},{48,56},{56,64},{64,7... | collective-permute-start | bytes 393224 | tf_op jit(solution)/shard_map/ppermute | solution.py:37
  68.3 7.4 %collective-permute-start.29 = (bf16[64,1024]{1,0:T(8,128)(2,1)S(1)}, bf16[64,1024]{1,0:T(8,128)(2,1)S(1)}, u32[]{:S(2)}, u32[]{:S(2)}) collective-permute-start(bf16[64,1024]{1,0:T(8,128)(2,1)S(1)} %collective-permute-done.28.refs_35_), channel_id=1, source_target_pairs={{0,8},{8,16},{16,24},{24,32},{32,40},{40,48},{48,56},{56,64},{64,7... | collective-permute-start | bytes 393224 | tf_op jit(solution)/shard_map/ppermute | solution.py:37
  74.3 6.2 %collective-permute-start.22 = (bf16[64,1024]{1,0:T(8,128)(2,1)S(1)}, bf16[64,1024]{1,0:T(8,128)(2,1)S(1)}, u32[]{:S(2)}, u32[]{:S(2)}) collective-permute-start(bf16[64,1024]{1,0:T(8,128)(2,1)S(1)} %collective-permute-done.21.refs_22_), channel_id=1, source_target_pairs={{0,120},{8,0},{16,8},{24,16},{32,24},{40,32},{48,40},{56,48},{64,5... | collective-permute-start | bytes 393224 | tf_op jit(solution)/shard_map/ppermute | solution.py:37
  75.7 6.9 %collective-permute-start.14 = (bf16[64,1024]{1,0:T(8,128)(2,1)S(1)}, bf16[64,1024]{1,0:T(8,128)(2,1)S(1)}, u32[]{:S(2)}, u32[]{:S(2)}) collective-permute-start(bf16[64,1024]{1,0:T(8,128)(2,1)S(1)} %collective-permute-done.13.refs_17_), channel_id=1, source_target_pairs={{0,8},{8,16},{16,24},{24,32},{32,40},{40,48},{48,56},{56,64},{64,7... | collective-permute-start | bytes 393224 | tf_op jit(solution)/shard_map/ppermute | solution.py:37
  76.9 6.4 %collective-permute-start.30 = (bf16[64,1024]{1,0:T(8,128)(2,1)S(1)}, bf16[64,1024]{1,0:T(8,128)(2,1)S(1)}, u32[]{:S(2)}, u32[]{:S(2)}) collective-permute-start(bf16[64,1024]{1,0:T(8,128)(2,1)S(1)} %collective-permute-done.29.refs_34_), channel_id=1, source_target_pairs={{0,8},{8,16},{16,24},{24,32},{32,40},{40,48},{48,56},{56,64},{64,7... | collective-permute-start | bytes 393224 | tf_op jit(solution)/shard_map/ppermute | solution.py:37
  82.6 6.4 %collective-permute-start.23 = (bf16[64,1024]{1,0:T(8,128)(2,1)S(1)}, bf16[64,1024]{1,0:T(8,128)(2,1)S(1)}, u32[]{:S(2)}, u32[]{:S(2)}) collective-permute-start(bf16[64,1024]{1,0:T(8,128)(2,1)S(1)} %collective-permute-done.22.refs_23_), channel_id=1, source_target_pairs={{0,120},{8,0},{16,8},{24,16},{32,24},{40,32},{48,40},{56,48},{64,5... | collective-permute-start | bytes 393224 | tf_op jit(solution)/shard_map/ppermute | solution.py:37
  83.3 8.8 %collective-permute-start.15 = (bf16[64,1024]{1,0:T(8,128)(2,1)S(1)}, bf16[64,1024]{1,0:T(8,128)(2,1)S(1)}, u32[]{:S(2)}, u32[]{:S(2)}) collective-permute-start(bf16[64,1024]{1,0:T(8,128)(2,1)S(1)} %collective-permute-done.14.refs_16_), channel_id=1, source_target_pairs={{0,8},{8,16},{16,24},{24,32},{32,40},{40,48},{48,56},{56,64},{64,7... | collective-permute-start | bytes 393224 | tf_op jit(solution)/shard_map/ppermute | solution.py:37
  86.1 7.3 %collective-permute-start.31 = (bf16[64,1024]{1,0:T(8,128)(2,1)S(1)}, bf16[64,1024]{1,0:T(8,128)(2,1)S(1)}, u32[]{:S(2)}, u32[]{:S(2)}) collective-permute-start(bf16[64,1024]{1,0:T(8,128)(2,1)S(1)} %collective-permute-done.30.refs_33_), channel_id=1, source_target_pairs={{0,8},{8,16},{16,24},{24,32},{32,40},{40,48},{48,56},{56,64},{64,7... | collective-permute-start | bytes 393224 | tf_op jit(solution)/shard_map/ppermute | solution.py:37
  89.0 7.1 %collective-permute-start.8 = (bf16[64,1024]{1,0:T(8,128)(2,1)S(1)}, bf16[64,1024]{1,0:T(8,128)(2,1)S(1)}, u32[]{:S(2)}, u32[]{:S(2)}) collective-permute-start(bf16[64,1024]{1,0:T(8,128)(2,1)S(1)} %collective-permute-done.7.refs_8_), channel_id=1, source_target_pairs={{0,120},{8,0},{16,8},{24,16},{32,24},{40,32},{48,40},{56,48},{64,5... | collective-permute-start | bytes 393224 | tf_op jit(solution)/shard_map/ppermute | solution.py:37
  92.2 6.4 %collective-permute-start.24 = (bf16[64,1024]{1,0:T(8,128)(2,1)S(1)}, bf16[64,1024]{1,0:T(8,128)(2,1)S(1)}, u32[]{:S(2)}, u32[]{:S(2)}) collective-permute-start(bf16[64,1024]{1,0:T(8,128)(2,1)S(1)} %collective-permute-done.23.refs_24_), channel_id=1, source_target_pairs={{0,120},{8,0},{16,8},{24,16},{32,24},{40,32},{48,40},{56,48},{64,5... | collective-permute-start | bytes 393224 | tf_op jit(solution)/shard_map/ppermute | solution.py:37
  93.4 8.9 %collective-permute-start.16 = (bf16[64,1024]{1,0:T(8,128)(2,1)S(1)}, bf16[64,1024]{1,0:T(8,128)(2,1)S(1)}, u32[]{:S(2)}, u32[]{:S(2)}) collective-permute-start(bf16[64,1024]{1,0:T(8,128)(2,1)S(1)} %collective-permute-done.15.refs_15_), channel_id=1, source_target_pairs={{0,8},{8,16},{16,24},{24,32},{32,40},{40,48},{48,56},{56,64},{64,7... | collective-permute-start | bytes 393224 | tf_op jit(solution)/shard_map/ppermute | solution.py:37
  96.0 7.3 %collective-permute-start.32 = (bf16[64,1024]{1,0:T(8,128)(2,1)S(1)}, bf16[64,1024]{1,0:T(8,128)(2,1)S(1)}, u32[]{:S(2)}, u32[]{:S(2)}) collective-permute-start(bf16[64,1024]{1,0:T(8,128)(2,1)S(1)} %collective-permute-done.31.refs_32_), channel_id=1, source_target_pairs={{0,8},{8,16},{16,24},{24,32},{32,40},{40,48},{48,56},{56,64},{64,7... | collective-permute-start | bytes 393224 | tf_op jit(solution)/shard_map/ppermute | solution.py:37
  98.5 7.6 %collective-permute-start.9 = (bf16[64,1024]{1,0:T(8,128)(2,1)S(1)}, bf16[64,1024]{1,0:T(8,128)(2,1)S(1)}, u32[]{:S(2)}, u32[]{:S(2)}) collective-permute-start(bf16[64,1024]{1,0:T(8,128)(2,1)S(1)} %collective-permute-done.8.refs_9_), channel_id=1, source_target_pairs={{0,120},{8,0},{16,8},{24,16},{32,24},{40,32},{48,40},{56,48},{64,5... | collective-permute-start | bytes 393224 | tf_op jit(solution)/shard_map/ppermute | solution.py:37
  103.3 8.2 %collective-permute-start.17 = (bf16[64,1024]{1,0:T(8,128)(2,1)S(1)}, bf16[64,1024]{1,0:T(8,128)(2,1)S(1)}, u32[]{:S(2)}, u32[]{:S(2)}) collective-permute-start(bf16[64,1024]{1,0:T(8,128)(2,1)S(1)} %collective-permute-done.16.refs_14_), channel_id=1, source_target_pairs={{0,8},{8,16},{16,24},{24,32},{32,40},{40,48},{48,56},{56,64},{64,7... | collective-permute-start | bytes 393224 | tf_op jit(solution)/shard_map/ppermute | solution.py:37
  106.1 7.9 %collective-permute-start.33 = (bf16[64,1024]{1,0:T(8,128)(2,1)S(1)}, bf16[64,1024]{1,0:T(8,128)(2,1)S(1)}, u32[]{:S(2)}, u32[]{:S(2)}) collective-permute-start(bf16[64,1024]{1,0:T(8,128)(2,1)S(1)} %collective-permute-done.32.refs_31_), channel_id=1, source_target_pairs={{0,8},{8,16},{16,24},{24,32},{32,40},{40,48},{48,56},{56,64},{64,7... | collective-permute-start | bytes 393224 | tf_op jit(solution)/shard_map/ppermute | solution.py:37
  108.1 7.7 %collective-permute-start.10 = (bf16[64,1024]{1,0:T(8,128)(2,1)S(1)}, bf16[64,1024]{1,0:T(8,128)(2,1)S(1)}, u32[]{:S(2)}, u32[]{:S(2)}) collective-permute-start(bf16[64,1024]{1,0:T(8,128)(2,1)S(1)} %collective-permute-done.9.refs_10_), channel_id=1, source_target_pairs={{0,120},{8,0},{16,8},{24,16},{32,24},{40,32},{48,40},{56,48},{64,5... | collective-permute-start | bytes 393224 | tf_op jit(solution)/shard_map/ppermute | solution.py:37
  111.5 15.5 %collective-permute-start.3 = (bf16[384,512]{1,0:T(8,128)(2,1)S(1)}, bf16[384,512]{1,0:T(8,128)(2,1)S(1)}, u32[]{:S(2)}, u32[]{:S(2)}) collective-permute-start(bf16[384,512]{1,0:T(8,128)(2,1)S(1)} %slice.4), channel_id=1, source_target_pairs={{0,2},{2,4},{4,6},{6,0},{1,3},{3,5},{5,7},{7,1},{8,10},{10,12},{12... | collective-permute-start | bytes 1179656 | tf_op jit(solution)/shard_map/ppermute | solution.py:37
  134.3 13.5 %collective-permute-start.37 = (bf16[1408,512]{1,0:T(8,128)(2,1)S(1)}, bf16[1408,512]{1,0:T(8,128)(2,1)}, u32[]{:S(2)}, u32[]{:S(2)}) collective-permute-start(bf16[1408,512]{1,0:T(8,128)(2,1)S(1)} %pack.1.refs_0_), channel_id=1, source_target_pairs={{0,1},{1,0},{2,3},{3,2},{4,5},{5,4},{6,7},{7,6},{8,9},{9,8},{10,11... | collective-permute-start | bytes 4325384 | tf_op jit(solution)/shard_map/ppermute | solution.py:41
  134.8 13.0 %collective-permute-start.40 = (bf16[1408,512]{1,0:T(8,128)(2,1)S(1)}, bf16[1408,512]{1,0:T(8,128)(2,1)}, u32[]{:S(2)}, u32[]{:S(2)}) collective-permute-start(bf16[1408,512]{1,0:T(8,128)(2,1)S(1)} %collective-permute-done.2.refs_3_), channel_id=1, source_target_pairs={{0,1},{1,0},{2,3},{3,2},{4,5},{5,4},{6,7},{7,6},{8,9},{9,8},{10,11... | collective-permute-start | bytes 4325384 | tf_op jit(solution)/shard_map/ppermute | solution.py:41
  134.9 12.8 %collective-permute-start.38 = (bf16[1408,512]{1,0:T(8,128)(2,1)}, bf16[1408,512]{1,0:T(8,128)(2,1)}, u32[]{:S(2)}, u32[]{:S(2)}) collective-permute-start(bf16[1408,512]{1,0:T(8,128)(2,1)} %collective-permute-done.1.refs_1_), channel_id=1, source_target_pairs={{0,1},{1,0},{2,3},{3,2},{4,5},{5,4},{6,7},{7,6},{8,9},{9,8},{10,11... | collective-permute-start | bytes 4325384 | tf_op jit(solution)/shard_map/ppermute | solution.py:41
  135.3 30.7 %collective-permute-start.39 = (bf16[1408,512]{1,0:T(8,128)(2,1)}, bf16[1408,512]{1,0:T(8,128)(2,1)}, u32[]{:S(2)}, u32[]{:S(2)}) collective-permute-start(bf16[1408,512]{1,0:T(8,128)(2,1)} %collective-permute-done.36.refs_2_), channel_id=1, source_target_pairs={{0,1},{1,0},{2,3},{3,2},{4,5},{5,4},{6,7},{7,6},{8,9},{9,8},{10,11... | collective-permute-start | bytes 4325384 | tf_op jit(solution)/shard_map/ppermute | solution.py:41
  143.8 22.2 %all-to-all-start = ((bf16[16,64,128]{2,1,0:T(8,128)(2,1)}), bf16[16,64,128]{2,1,0:T(8,128)(2,1)S(1)}, u32[]{:S(2)}, u32[]{:S(2)}) async-start(bf16[16,64,128]{2,1,0:T(8,128)(2,1)} %mixer.1), calls=%async_computation | async-start | bytes 524288 | tf_op jit(solution)/shard_map/all_to_all | solution.py:451
  (15 other events, 437.9 us)
where the time goes:
time: 172 us
  starting transfers between devices  81.2 us (47%)
  waiting for transfers between devices  67.3 us (39%)
  Pallas kernels  22.9 us (13%)
    ppermute x34, starting transfers between devices, shift(): return lax.ppermute(x, axis, ring(lax.axis_size(axis), step))  75.6 us
    ppermute x34, waiting for transfers between devices, shift(): return lax.ppermute(x, axis, ring(lax.axis_size(axis), step))  46.7 us
    all_to_all x1, waiting for transfers between devices, body(): lax.all_to_all(mixed_heads, 'sp', split_axis=0, concat_axis=0, tiled=True)  18.2 us
    pallas_call x1, Pallas kernels, body(): pl.pallas_call(mixer_kernel, out_shape=jax.ShapeDtypeStruct((sp, rows, HE...  7.58 us
    pallas_call x1, Pallas kernels, body(): pl.pallas_call(project_kernel, out_shape=(jax.ShapeDtypeStruct((sp * rows...  7.14 us
    pallas_call x1, Pallas kernels, body(): pl.pallas_call(output_kernel, out_shape=jax.ShapeDtypeStruct((rows, fs *...  5.76 us
    all_to_all x1, starting transfers between devices, body(): lax.all_to_all(mixed_heads, 'sp', split_axis=0, concat_axis=0, tiled=True)  3.97 us
  transfers between devices with their start and end apart: 42, of which 24 were waited for; matrix products, arithmetic and copies ran while one was open for 0% of the time, Pallas kernels for 9%

commit v1 on v0

--- a/solution.py
+++ b/solution.py
@@ -1,3 +1,4 @@
+import functools
 import math
 
 import jax
@@ -91,10 +92,14 @@
         copy.wait()
 
 
-def project_kernel(gain_ref, offset_ref, room_ref, *refs):
+def project_kernel(done, gain_ref, offset_ref, room_ref, *refs):
     fs = lax.axis_size("fs")
+    query_ref, pair_ref, norm_ref = refs[-3:]
+    if done:
+        query_ref[0:done, :] = refs[0][...]
+        pair_ref[0:done, :] = refs[1][...]
+        refs = refs[2:]
     packs, refs = refs[:fs], refs[fs:]
-    query_ref, pair_ref, norm_ref = refs[-3:]
     count = (len(refs) - 3) // 2
     near, far = refs[:count], refs[count : 2 * count]
     rows, half = near[0].shape
@@ -117,7 +122,7 @@
         norm_ref[own, :] = (value * factor * gain).astype(bf16)
         return 0
 
-    lax.fori_loop(0, count, normalize, 0, unroll=2)
+    lax.fori_loop(0, count, normalize, 0)
     group = 4 * rows
 
     def multiply(k, _):
@@ -127,20 +132,23 @@
             at = pl.ds(pl.multiple_of((x + step) % fs * each, each), each)
             product += mm_t(norm_ref[own, at], packs[step][packs[step].shape[0] - 3 * HEAD :, :])
         product = product.astype(bf16)
-        query_ref[own, :] = product[:, :HEAD]
-        pair_ref[own, :] = product[:, HEAD:]
+        to = pl.ds(pl.multiple_of(done + k * group, group), group)
+        query_ref[to, :] = product[:, :HEAD]
+        pair_ref[to, :] = product[:, HEAD:]
         return 0
 
     lax.fori_loop(0, count * rows // group, multiply, 0)
+    if not done:
+        return
     offset = jnp.full((1, HEAD), offset_ref[local], f32)
     rest = jnp.concatenate([room_ref[pl.ds(local, 1), :], offset], 1)
     parts = []
     for _ in range(3):
         parts.append(rest.astype(bf16).astype(f32))
         rest = rest - parts[-1]
-    extra = pair_ref.shape[0] - count * rows
-    pad = jnp.zeros((extra - 3, 2 * HEAD), f32)
-    pair_ref[count * rows :, :] = jnp.concatenate(parts + [pad], 0).astype(bf16)
+    used = done + count * rows
+    pad = jnp.zeros((PARAM_ROWS - 3, 2 * HEAD), f32)
+    pair_ref[used : used + PARAM_ROWS, :] = jnp.concatenate(parts + [pad], 0).astype(bf16)
 
 
 def stick_body(half, offset, q_ref, kv_ref, sums_ref, out_ref, acc_ref, carry_ref, rows, blocks):
@@ -247,14 +255,19 @@
     span = 2 * rows
     place, half = lax.axis_index("sp"), lax.axis_index("tp")
     head, _, is_attn = place_of_head()
-    for k in range(blocks):
-        block = (place + k) % blocks
-        own = slice(k * rows, (k + 1) * rows)
+
+    def settle(k, _):
+        slot = jnp.where(k < 7, k, jnp.where(k < MOST, 22 - k, k - 5))
+        block = (place + slot) % blocks
+        own = pl.ds(pl.multiple_of(k * rows, rows), rows)
         q_ref[pl.ds(pl.multiple_of(block * rows, rows), rows), :] = query_ref[own, :]
         at = pl.multiple_of((2 * block + half) * rows, rows)
         kv_ref[pl.ds(at, rows), :] = mine_ref[own, :]
         at = pl.multiple_of((2 * block + 1 - half) * rows, rows)
         kv_ref[pl.ds(at, rows), :] = other_ref[own, :]
+        return 0
+
+    lax.fori_loop(0, blocks, settle, 0)
     used = blocks * rows
     holds = holder_of(head) == half
     parts = jnp.where(
@@ -303,6 +316,8 @@
         out_ref[:, pl.ds(at, width)] = total.astype(bf16)
 
 
+SLOTS = (0, 1, 2, 3, 4, 5, 6, 15, 14, 13, 12, 11, 7, 8, 9, 10)
+MOST = 12
 PARAM_ROWS = 16
 
 MIB = 1 << 20
@@ -409,25 +424,32 @@
                 behind[k] = shift(behind[k], "sp", -1)
                 store[hop] = behind[k]
 
-    query, pair = pl.pallas_call(
-        project_kernel,
-        out_shape=(
-            jax.ShapeDtypeStruct((sp * rows, HEAD), bf16),
-            jax.ShapeDtypeStruct((sp * rows + PARAM_ROWS, 2 * HEAD), bf16),
-        ),
-        in_specs=[whole, scalar] + [whole] * (1 + fs + 2 * sp),
-        out_specs=(whole, whole),
-        scratch_shapes=[pltpu.VMEM((sp * rows, 2 * half_width), bf16)],
-        compiler_params=limit(12),
-        name="project",
-    )(
-        mix_gain[None, :],
-        break_offset,
-        forget_room,
-        *resident([pack, from_next, far_columns, from_prev]),
-        *resident([near_blocks[s] for s in range(sp)]),
-        *resident([far_blocks[s] for s in range(sp)]),
-    )
+    def project(done, slots, earlier):
+        count = len(slots) * rows
+        extra = PARAM_ROWS if done else 0
+        return pl.pallas_call(
+            functools.partial(project_kernel, done),
+            out_shape=(
+                jax.ShapeDtypeStruct((done + count, HEAD), bf16),
+                jax.ShapeDtypeStruct((done + count + extra, 2 * HEAD), bf16),
+            ),
+            in_specs=[whole, scalar] + [whole] * (1 + len(earlier) + fs + 2 * len(slots)),
+            out_specs=(whole, whole),
+            scratch_shapes=[pltpu.VMEM((count, 2 * half_width), bf16)],
+            compiler_params=limit(12),
+            name="project",
+        )(
+            mix_gain[None, :],
+            break_offset,
+            forget_room,
+            *resident(earlier),
+            *resident([pack, from_next, far_columns, from_prev]),
+            *resident([near_blocks[s] for s in slots]),
+            *resident([far_blocks[s] for s in slots]),
+        )
+
+    most = project(0, SLOTS[:MOST], [])
+    query, pair = project(MOST * rows, SLOTS[MOST:], most)
     pair_other = swap(pair)
 
     span = rows * tp

time: 172 us -> 172 us (level)
  the two profiles are of different devices: /device:TPU:46 before, /device:TPU:40 now
where the time goes in v1:
time: 172 us; the launch traced here: 171 us
  starting transfers between devices  89.1 us (52%)
  waiting for transfers between devices  57.4 us (33%)
  Pallas kernels  24.5 us (14%)
    ppermute x34, starting transfers between devices, shift(): return lax.ppermute(x, axis, ring(lax.axis_size(axis), step))  82.4 us
    ppermute x34, waiting for transfers between devices, shift(): return lax.ppermute(x, axis, ring(lax.axis_size(axis), step))  36.7 us
    all_to_all x1, waiting for transfers between devices, body(): lax.all_to_all(mixed_heads, 'sp', split_axis=0, concat_axis=0, tiled=True)  18.3 us
    pallas_call x2, Pallas kernels, project(): pl.pallas_call(functools.partial(project_kernel, done), out_shape=(jax.Sh...  8.64 us
    pallas_call x1, Pallas kernels, body(): pl.pallas_call(mixer_kernel, out_shape=jax.ShapeDtypeStruct((sp, rows, HE...  7.64 us
    pallas_call x1, Pallas kernels, body(): pl.pallas_call(output_kernel, out_shape=jax.ShapeDtypeStruct((rows, fs *...  5.76 us
    all_to_all x1, starting transfers between devices, body(): lax.all_to_all(mixed_heads, 'sp', split_axis=0, concat_axis=0, tiled=True)  5.15 us
  transfers between devices with their start and end apart: 42, of which 20 were waited for; matrix products, arithmetic and copies ran while one was open for 0% of the time, Pallas kernels for 10%

profile of v1, /device:TPU:40, one launch (start us, length us, event | category | flops | bytes accessed | tf_op | source)
XLA Modules:
  0.0 171.3 jit_solution(9165020744594575109)
XLA Ops:
  1.4 1.7 collective-permute-done.other_ref
  4.3 1.7 %collective-permute-start.2 = (bf16[1408,512]{1,0:T(8,128)(2,1)S(1)}, bf16[1408,512]{1,0:T(8,128)(2,1)S(1)}, u32[]{:S(2)}, u32[]{:S(2)}) collective-permute-start(bf16[1408,512]{1,0:T(8,128)(2,1)S(1)} %pack.1.refs_0_.refs_2_), channel_id=1, source_target_pairs={{0,2},{2,4},{4,6},{6,0},{1,3},{3,5},{5,7},{7,1},{8,10},{10,12},{12... | collective-permute-start | bytes 4325384 | tf_op jit(solution)/shard_map/ppermute | solution.py:38
  6.1 1.7 collective-permute-start.1
  7.9 22.5 %collective-permute-start.4 = (bf16[64,1024]{1,0:T(8,128)(2,1)S(1)}, bf16[64,1024]{1,0:T(8,128)(2,1)S(1)}, u32[]{:S(2)}, u32[]{:S(2)}) collective-permute-start(bf16[64,1024]{1,0:T(8,128)(2,1)S(1)} %get-tuple-element.14.refs_4_), channel_id=1, source_target_pairs={{0,120},{8,0},{16,8},{24,16},{32,24},{40,32},{48,40},{56,48},{64,5... | collective-permute-start | bytes 393224 | tf_op jit(solution)/shard_map/ppermute | solution.py:38
  30.4 9.1 %collective-permute-done.2.refs_3_.refs_5_ = bf16[1408,512]{1,0:T(8,128)(2,1)S(1)} collective-permute-done((bf16[1408,512]{1,0:T(8,128)(2,1)S(1)}, bf16[1408,512]{1,0:T(8,128)(2,1)S(1)}, u32[]{:S(2)}, u32[]{:S(2)}) %collective-permute-start.2) | collective-permute-done | bytes 1441824 | tf_op jit(solution)/shard_map/ppermute | solution.py:38
  39.7 22.4 %collective-permute-start.16 = (bf16[64,1024]{1,0:T(8,128)(2,1)S(1)}, bf16[64,1024]{1,0:T(8,128)(2,1)S(1)}, u32[]{:S(2)}, u32[]{:S(2)}) collective-permute-start(bf16[64,1024]{1,0:T(8,128)(2,1)S(1)} %collective-permute-done.15.refs_16_), channel_id=1, source_target_pairs={{0,120},{8,0},{16,8},{24,16},{32,24},{40,32},{48,40},{56,48},{64,5... | collective-permute-start | bytes 393224 | tf_op jit(solution)/shard_map/ppermute | solution.py:38
  62.2 1.9 %collective-permute-start.22 = (bf16[64,1024]{1,0:T(8,128)(2,1)S(1)}, bf16[64,1024]{1,0:T(8,128)(2,1)S(1)}, u32[]{:S(2)}, u32[]{:S(2)}) collective-permute-start(bf16[64,1024]{1,0:T(8,128)(2,1)S(1)} %collective-permute-done.15.refs_16_), channel_id=1, source_target_pairs={{0,8},{8,16},{16,24},{24,32},{32,40},{40,48},{48,56},{56,64},{64,7... | collective-permute-start | bytes 393224 | tf_op jit(solution)/shard_map/ppermute | solution.py:38
  64.1 1.6 collective-permute-done.16.refs_17_
  67.1 3.7 %collective-permute-start.17 = (bf16[64,1024]{1,0:T(8,128)(2,1)S(1)}, bf16[64,1024]{1,0:T(8,128)(2,1)S(1)}, u32[]{:S(2)}, u32[]{:S(2)}) collective-permute-start(bf16[64,1024]{1,0:T(8,128)(2,1)S(1)} %collective-permute-done.16.refs_17_), channel_id=1, source_target_pairs={{0,120},{8,0},{16,8},{24,16},{32,24},{40,32},{48,40},{56,48},{64,5... | collective-permute-start | bytes 393224 | tf_op jit(solution)/shard_map/ppermute | solution.py:38
  73.7 2.1 %collective-permute-done.6.refs_7_ = bf16[64,1024]{1,0:T(8,128)(2,1)S(1)} collective-permute-done((bf16[64,1024]{1,0:T(8,128)(2,1)S(1)}, bf16[64,1024]{1,0:T(8,128)(2,1)S(1)}, u32[]{:S(2)}, u32[]{:S(2)}) %collective-permute-start.6) | collective-permute-done | bytes 131104 | tf_op jit(solution)/shard_map/ppermute | solution.py:38
  75.8 3.0 %collective-permute-start.18 = (bf16[64,1024]{1,0:T(8,128)(2,1)S(1)}, bf16[64,1024]{1,0:T(8,128)(2,1)S(1)}, u32[]{:S(2)}, u32[]{:S(2)}) collective-permute-start(bf16[64,1024]{1,0:T(8,128)(2,1)S(1)} %collective-permute-done.17.refs_18_), channel_id=1, source_target_pairs={{0,120},{8,0},{16,8},{24,16},{32,24},{40,32},{48,40},{56,48},{64,5... | collective-permute-start | bytes 393224 | tf_op jit(solution)/shard_map/ppermute | solution.py:38
  78.8 1.7 collective-permute-start.7
  81.8 2.0 %collective-permute-done.7.refs_8_ = bf16[64,1024]{1,0:T(8,128)(2,1)S(1)} collective-permute-done((bf16[64,1024]{1,0:T(8,128)(2,1)S(1)}, bf16[64,1024]{1,0:T(8,128)(2,1)S(1)}, u32[]{:S(2)}, u32[]{:S(2)}) %collective-permute-start.7) | collective-permute-done | bytes 131104 | tf_op jit(solution)/shard_map/ppermute | solution.py:38
  83.8 2.9 %collective-permute-start.19 = (bf16[64,1024]{1,0:T(8,128)(2,1)S(1)}, bf16[64,1024]{1,0:T(8,128)(2,1)S(1)}, u32[]{:S(2)}, u32[]{:S(2)}) collective-permute-start(bf16[64,1024]{1,0:T(8,128)(2,1)S(1)} %collective-permute-done.18.refs_19_), channel_id=1, source_target_pairs={{0,120},{8,0},{16,8},{24,16},{32,24},{40,32},{48,40},{56,48},{64,5... | collective-permute-start | bytes 393224 | tf_op jit(solution)/shard_map/ppermute | solution.py:38
  86.7 1.4 collective-permute-start.8
  89.2 3.6 %collective-permute-done.8.refs_9_ = bf16[64,1024]{1,0:T(8,128)(2,1)S(1)} collective-permute-done((bf16[64,1024]{1,0:T(8,128)(2,1)S(1)}, bf16[64,1024]{1,0:T(8,128)(2,1)S(1)}, u32[]{:S(2)}, u32[]{:S(2)}) %collective-permute-start.8) | collective-permute-done | bytes 131104 | tf_op jit(solution)/shard_map/ppermute | solution.py:38
  92.8 1.6 collective-permute-start.20
  94.4 1.9 %collective-permute-start.9 = (bf16[64,1024]{1,0:T(8,128)(2,1)S(1)}, bf16[64,1024]{1,0:T(8,128)(2,1)S(1)}, u32[]{:S(2)}, u32[]{:S(2)}) collective-permute-start(bf16[64,1024]{1,0:T(8,128)(2,1)S(1)} %collective-permute-done.8.refs_9_), channel_id=1, source_target_pairs={{0,120},{8,0},{16,8},{24,16},{32,24},{40,32},{48,40},{56,48},{64,5... | collective-permute-start | bytes 393224 | tf_op jit(solution)/shard_map/ppermute | solution.py:38
  97.8 1.6 collective-permute-done.9.refs_10_
  99.4 4.9 %collective-permute-start.3 = (bf16[384,512]{1,0:T(8,128)(2,1)S(1)}, bf16[384,512]{1,0:T(8,128)(2,1)S(1)}, u32[]{:S(2)}, u32[]{:S(2)}) collective-permute-start(bf16[384,512]{1,0:T(8,128)(2,1)S(1)} %slice.4), channel_id=1, source_target_pairs={{0,2},{2,4},{4,6},{6,0},{1,3},{3,5},{5,7},{7,1},{8,10},{10,12},{12... | collective-permute-start | bytes 1179656 | tf_op jit(solution)/shard_map/ppermute | solution.py:38
  104.3 2.6 %collective-permute-start.21 = (bf16[64,1024]{1,0:T(8,128)(2,1)S(1)}, bf16[64,1024]{1,0:T(8,128)(2,1)S(1)}, u32[]{:S(2)}, u32[]{:S(2)}) collective-permute-start(bf16[64,1024]{1,0:T(8,128)(2,1)S(1)} %collective-permute-done.20.refs_21_), channel_id=1, source_target_pairs={{0,120},{8,0},{16,8},{24,16},{32,24},{40,32},{48,40},{56,48},{64,5... | collective-permute-start | bytes 393224 | tf_op jit(solution)/shard_map/ppermute | solution.py:38
  106.9 3.7 %collective-permute-done.21.refs_22_ = bf16[64,1024]{1,0:T(8,128)(2,1)S(1)} collective-permute-done((bf16[64,1024]{1,0:T(8,128)(2,1)S(1)}, bf16[64,1024]{1,0:T(8,128)(2,1)S(1)}, u32[]{:S(2)}, u32[]{:S(2)}) %collective-permute-start.21) | collective-permute-done | bytes 131104 | tf_op jit(solution)/shard_map/ppermute | solution.py:38
  110.6 2.4 %collective-permute-done.29.refs_8_ = bf16[64,1024]{1,0:T(8,128)(2,1)S(1)} collective-permute-done((bf16[64,1024]{1,0:T(8,128)(2,1)S(1)}, bf16[64,1024]{1,0:T(8,128)(2,1)S(1)}, u32[]{:S(2)}, u32[]{:S(2)}) %collective-permute-start.29) | collective-permute-done | bytes 131104 | tf_op jit(solution)/shard_map/ppermute | solution.py:38
  114.1 4.3 %collective-permute-done.33.refs_13_ = bf16[64,1024]{1,0:T(8,128)(2,1)S(1)} collective-permute-done((bf16[64,1024]{1,0:T(8,128)(2,1)S(1)}, bf16[64,1024]{1,0:T(8,128)(2,1)S(1)}, u32[]{:S(2)}, u32[]{:S(2)}) %collective-permute-start.33) | collective-permute-done | bytes 131104 | tf_op jit(solution)/shard_map/ppermute | solution.py:38
  119.0 1.4 collective-permute-start.30
  120.6 3.1 %collective-permute-start.32 = (bf16[64,1024]{1,0:T(8,128)(2,1)S(1)}, bf16[64,1024]{1,0:T(8,128)(2,1)S(1)}, u32[]{:S(2)}, u32[]{:S(2)}) collective-permute-start(bf16[64,1024]{1,0:T(8,128)(2,1)S(1)} %collective-permute-done.31.refs_10_), channel_id=1, source_target_pairs={{0,120},{8,0},{16,8},{24,16},{32,24},{40,32},{48,40},{56,48},{64,5... | collective-permute-start | bytes 393224 | tf_op jit(solution)/shard_map/ppermute | solution.py:38
  123.7 5.8 %project.2 = (bf16[768,128]{1,0:T(8,128)(2,1)S(1)}, bf16[768,256]{1,0:T(8,128)(2,1)S(1)}) custom-call(f32[1,2048]{1,0:T(1,128)S(1)} %bitcast.7, f32[4]{0:T(128)S(1)} %copy-done.2, f32[4,128]{1,0:T(4,128)S(1)} %copy-done.1, bf16[1408,512]{1,0:T(8,128)(2,1)S(1)} %pack.1.refs_0_.refs_2_, bf16[1408,512]{1,0:T(8,128)(2,1)} %collective-permute-done.1.refs_1_.refs_3_, ...), custom_call_target="tpu_custom_call" | custom-call | tf_op jit(solution)/shard_map/project/pallas_call | solution.py:430
  129.5 2.9 %project.3 = (bf16[1024,128]{1,0:T(8,128)(2,1)S(1)}, bf16[1040,256]{1,0:T(8,128)(2,1)S(1)}) custom-call(f32[1,2048]{1,0:T(1,128)S(1)} %bitcast.8, f32[4]{0:T(128)S(1)} %copy-done.2, f32[4,128]{1,0:T(4,128)S(1)} %copy-done.1, bf16[768,128]{1,0:T(8,128)(2,1)S(1)} %get-tuple-element.9.refs_0_, bf16[768,256]{1,0:T(8,128)(2,1)S(1)} %get-tuple-element.10.refs_1_, ...), custom_call_target="tpu_custom_call" | custom-call | tf_op jit(solution)/shard_map/project/pallas_call | solution.py:430
  134.5 7.6 %mixer.1 = bf16[16,64,128]{2,1,0:T(8,128)(2,1)} custom-call(f32[1,128]{1,0:T(1,128)S(1)} %bitcast.9, bf16[1024,128]{1,0:T(8,128)(2,1)S(1)} %get-tuple-element.11.query_ref, bf16[1040,256]{1,0:T(8,128)(2,1)S(1)} %get-tuple-element.12.mine_ref, bf16[1040,256]{1,0:T(8,128)(2,1)S(1)} %collective-permute-done.35.other_ref), custom_call_target="tpu_custom_call" | custom-call | tf_op jit(solution)/shard_map/mixer/pallas_call | solution.py:456
  142.1 5.1 %all-to-all-start = ((bf16[16,64,128]{2,1,0:T(8,128)(2,1)}), bf16[16,64,128]{2,1,0:T(8,128)(2,1)S(1)}, u32[]{:S(2)}, u32[]{:S(2)}) async-start(bf16[16,64,128]{2,1,0:T(8,128)(2,1)} %mixer.1), calls=%async_computation | async-start | bytes 524288 | tf_op jit(solution)/shard_map/all_to_all | solution.py:473
  147.3 18.3 %all-to-all-done.heads_ref = bf16[16,64,128]{2,1,0:T(8,128)(2,1)S(1)} async-done(((bf16[16,64,128]{2,1,0:T(8,128)(2,1)}), bf16[16,64,128]{2,1,0:T(8,128)(2,1)S(1)}, u32[]{:S(2)}, u32[]{:S(2)}) %all-to-all-start) | async-done | bytes 262176 | tf_op jit(solution)/shard_map/all_to_all | solution.py:473
  165.6 5.8 %output.1 = bf16[64,2048]{1,0:T(8,128)(2,1)} custom-call(bf16[16,64,128]{2,1,0:T(8,128)(2,1)S(1)} %all-to-all-done.heads_ref, bf16[1408,512]{1,0:T(8,128)(2,1)S(1)} %pack.1.refs_0_.refs_2_, bf16[1408,512]{1,0:T(8,128)(2,1)} %collective-permute-done.1.refs_1_.refs_3_, bf16[1408,512]{1,0:T(8,128)(2,1)} %collective-permute-done.36.refs_2_, ...), custom_call_target="tpu_custom_call" | custom-call | tf_op jit(solution)/shard_map/output/pallas_call | solution.py:474
  (70 shorter events, 15.0 us)
Async XLA Ops:
  4.3 35.2 %collective-permute-start.2 = (bf16[1408,512]{1,0:T(8,128)(2,1)S(1)}, bf16[1408,512]{1,0:T(8,128)(2,1)S(1)}, u32[]{:S(2)}, u32[]{:S(2)}) collective-permute-start(bf16[1408,512]{1,0:T(8,128)(2,1)S(1)} %pack.1.refs_0_.refs_2_), channel_id=1, source_target_pairs={{0,2},{2,4},{4,6},{6,0},{1,3},{3,5},{5,7},{7,1},{8,10},{10,12},{12... | collective-permute-start | bytes 4325384 | tf_op jit(solution)/shard_map/ppermute | solution.py:38
  6.1 114.4 %collective-permute-start.1 = (bf16[1408,512]{1,0:T(8,128)(2,1)S(1)}, bf16[1408,512]{1,0:T(8,128)(2,1)}, u32[]{:S(2)}, u32[]{:S(2)}) collective-permute-start(bf16[1408,512]{1,0:T(8,128)(2,1)S(1)} %pack.1.refs_0_.refs_2_), channel_id=1, source_target_pairs={{0,6},{2,0},{4,2},{6,4},{1,7},{3,1},{5,3},{7,5},{8,14},{10,8},{12,... | collective-permute-start | bytes 4325384 | tf_op jit(solution)/shard_map/ppermute | solution.py:38
  7.8 31.9 %collective-permute-start.15 = (bf16[64,1024]{1,0:T(8,128)(2,1)S(1)}, bf16[64,1024]{1,0:T(8,128)(2,1)S(1)}, u32[]{:S(2)}, u32[]{:S(2)}) collective-permute-start(bf16[64,1024]{1,0:T(8,128)(2,1)S(1)} %get-tuple-element.13), channel_id=1, source_target_pairs={{0,1},{1,0},{2,3},{3,2},{4,5},{5,4},{6,7},{7,6},{8,9},{9,8},{10,11... | collective-permute-start | bytes 393224 | tf_op jit(solution)/shard_map/ppermute | solution.py:42
  7.9 54.2 %collective-permute-start.4 = (bf16[64,1024]{1,0:T(8,128)(2,1)S(1)}, bf16[64,1024]{1,0:T(8,128)(2,1)S(1)}, u32[]{:S(2)}, u32[]{:S(2)}) collective-permute-start(bf16[64,1024]{1,0:T(8,128)(2,1)S(1)} %get-tuple-element.14.refs_4_), channel_id=1, source_target_pairs={{0,120},{8,0},{16,8},{24,16},{32,24},{40,32},{48,40},{56,48},{64,5... | collective-permute-start | bytes 393224 | tf_op jit(solution)/shard_map/ppermute | solution.py:38
  30.4 31.8 %collective-permute-start.10 = (bf16[64,1024]{1,0:T(8,128)(2,1)S(1)}, bf16[64,1024]{1,0:T(8,128)(2,1)S(1)}, u32[]{:S(2)}, u32[]{:S(2)}) collective-permute-start(bf16[64,1024]{1,0:T(8,128)(2,1)S(1)} %get-tuple-element.14.refs_4_), channel_id=1, source_target_pairs={{0,8},{8,16},{16,24},{24,32},{32,40},{40,48},{48,56},{56,64},{64,7... | collective-permute-start | bytes 393224 | tf_op jit(solution)/shard_map/ppermute | solution.py:38
  39.5 94.0 %collective-permute-start.36 = (bf16[1408,512]{1,0:T(8,128)(2,1)S(1)}, bf16[1408,512]{1,0:T(8,128)(2,1)}, u32[]{:S(2)}, u32[]{:S(2)}) collective-permute-start(bf16[1408,512]{1,0:T(8,128)(2,1)S(1)} %collective-permute-done.2.refs_3_.refs_5_), channel_id=1, source_target_pairs={{0,2},{2,4},{4,6},{6,0},{1,3},{3,5},{5,7},{7,1},{8,10},{10,12},{12... | collective-permute-start | bytes 4325384 | tf_op jit(solution)/shard_map/ppermute | solution.py:38
  39.7 26.0 %collective-permute-start.16 = (bf16[64,1024]{1,0:T(8,128)(2,1)S(1)}, bf16[64,1024]{1,0:T(8,128)(2,1)S(1)}, u32[]{:S(2)}, u32[]{:S(2)}) collective-permute-start(bf16[64,1024]{1,0:T(8,128)(2,1)S(1)} %collective-permute-done.15.refs_16_), channel_id=1, source_target_pairs={{0,120},{8,0},{16,8},{24,16},{32,24},{40,32},{48,40},{56,48},{64,5... | collective-permute-start | bytes 393224 | tf_op jit(solution)/shard_map/ppermute | solution.py:38
  62.2 8.6 %collective-permute-start.22 = (bf16[64,1024]{1,0:T(8,128)(2,1)S(1)}, bf16[64,1024]{1,0:T(8,128)(2,1)S(1)}, u32[]{:S(2)}, u32[]{:S(2)}) collective-permute-start(bf16[64,1024]{1,0:T(8,128)(2,1)S(1)} %collective-permute-done.15.refs_16_), channel_id=1, source_target_pairs={{0,8},{8,16},{16,24},{24,32},{32,40},{40,48},{48,56},{56,64},{64,7... | collective-permute-start | bytes 393224 | tf_op jit(solution)/shard_map/ppermute | solution.py:38
  65.7 6.6 %collective-permute-start.11 = (bf16[64,1024]{1,0:T(8,128)(2,1)S(1)}, bf16[64,1024]{1,0:T(8,128)(2,1)S(1)}, u32[]{:S(2)}, u32[]{:S(2)}) collective-permute-start(bf16[64,1024]{1,0:T(8,128)(2,1)S(1)} %collective-permute-done.10.refs_11_), channel_id=1, source_target_pairs={{0,8},{8,16},{16,24},{24,32},{32,40},{40,48},{48,56},{56,64},{64,7... | collective-permute-start | bytes 393224 | tf_op jit(solution)/shard_map/ppermute | solution.py:38
  67.1 6.6 %collective-permute-start.17 = (bf16[64,1024]{1,0:T(8,128)(2,1)S(1)}, bf16[64,1024]{1,0:T(8,128)(2,1)S(1)}, u32[]{:S(2)}, u32[]{:S(2)}) collective-permute-start(bf16[64,1024]{1,0:T(8,128)(2,1)S(1)} %collective-permute-done.16.refs_17_), channel_id=1, source_target_pairs={{0,120},{8,0},{16,8},{24,16},{32,24},{40,32},{48,40},{56,48},{64,5... | collective-permute-start | bytes 393224 | tf_op jit(solution)/shard_map/ppermute | solution.py:38
  72.4 6.5 %collective-permute-start.23 = (bf16[64,1024]{1,0:T(8,128)(2,1)S(1)}, bf16[64,1024]{1,0:T(8,128)(2,1)S(1)}, u32[]{:S(2)}, u32[]{:S(2)}) collective-permute-start(bf16[64,1024]{1,0:T(8,128)(2,1)S(1)} %collective-permute-done.22.refs_23_), channel_id=1, source_target_pairs={{0,8},{8,16},{16,24},{24,32},{32,40},{40,48},{48,56},{56,64},{64,7... | collective-permute-start | bytes 393224 | tf_op jit(solution)/shard_map/ppermute | solution.py:38
  73.7 6.8 %collective-permute-start.12 = (bf16[64,1024]{1,0:T(8,128)(2,1)S(1)}, bf16[64,1024]{1,0:T(8,128)(2,1)S(1)}, u32[]{:S(2)}, u32[]{:S(2)}) collective-permute-start(bf16[64,1024]{1,0:T(8,128)(2,1)S(1)} %collective-permute-done.11.refs_12_), channel_id=1, source_target_pairs={{0,8},{8,16},{16,24},{24,32},{32,40},{40,48},{48,56},{56,64},{64,7... | collective-permute-start | bytes 393224 | tf_op jit(solution)/shard_map/ppermute | solution.py:38
  80.5 6.2 %collective-permute-start.24 = (bf16[64,1024]{1,0:T(8,128)(2,1)S(1)}, bf16[64,1024]{1,0:T(8,128)(2,1)S(1)}, u32[]{:S(2)}, u32[]{:S(2)}) collective-permute-start(bf16[64,1024]{1,0:T(8,128)(2,1)S(1)} %collective-permute-done.23.refs_24_), channel_id=1, source_target_pairs={{0,8},{8,16},{16,24},{24,32},{32,40},{40,48},{48,56},{56,64},{64,7... | collective-permute-start | bytes 393224 | tf_op jit(solution)/shard_map/ppermute | solution.py:38
  81.8 6.5 %collective-permute-start.13 = (bf16[64,1024]{1,0:T(8,128)(2,1)S(1)}, bf16[64,1024]{1,0:T(8,128)(2,1)S(1)}, u32[]{:S(2)}, u32[]{:S(2)}) collective-permute-start(bf16[64,1024]{1,0:T(8,128)(2,1)S(1)} %collective-permute-done.12.refs_13_), channel_id=1, source_target_pairs={{0,8},{8,16},{16,24},{24,32},{32,40},{40,48},{48,56},{56,64},{64,7... | collective-permute-start | bytes 393224 | tf_op jit(solution)/shard_map/ppermute | solution.py:38
  86.7 6.1 %collective-permute-start.8 = (bf16[64,1024]{1,0:T(8,128)(2,1)S(1)}, bf16[64,1024]{1,0:T(8,128)(2,1)S(1)}, u32[]{:S(2)}, u32[]{:S(2)}) collective-permute-start(bf16[64,1024]{1,0:T(8,128)(2,1)S(1)} %collective-permute-done.7.refs_8_), channel_id=1, source_target_pairs={{0,120},{8,0},{16,8},{24,16},{32,24},{40,32},{48,40},{56,48},{64,5... | collective-permute-start | bytes 393224 | tf_op jit(solution)/shard_map/ppermute | solution.py:38
  88.2 6.2 %collective-permute-start.25 = (bf16[64,1024]{1,0:T(8,128)(2,1)S(1)}, bf16[64,1024]{1,0:T(8,128)(2,1)S(1)}, u32[]{:S(2)}, u32[]{:S(2)}) collective-permute-start(bf16[64,1024]{1,0:T(8,128)(2,1)S(1)} %collective-permute-done.24.refs_25_), channel_id=1, source_target_pairs={{0,8},{8,16},{16,24},{24,32},{32,40},{40,48},{48,56},{56,64},{64,7... | collective-permute-start | bytes 393224 | tf_op jit(solution)/shard_map/ppermute | solution.py:38
  89.2 7.3 %collective-permute-start.14 = (bf16[64,1024]{1,0:T(8,128)(2,1)S(1)}, bf16[64,1024]{1,0:T(8,128)(2,1)S(1)}, u32[]{:S(2)}, u32[]{:S(2)}) collective-permute-start(bf16[64,1024]{1,0:T(8,128)(2,1)S(1)} %collective-permute-done.13.refs_14_), channel_id=1, source_target_pairs={{0,8},{8,16},{16,24},{24,32},{32,40},{40,48},{48,56},{56,64},{64,7... | collective-permute-start | bytes 393224 | tf_op jit(solution)/shard_map/ppermute | solution.py:38
  96.5 7.8 %collective-permute-start.26 = (bf16[64,1024]{1,0:T(8,128)(2,1)S(1)}, bf16[64,1024]{1,0:T(8,128)(2,1)S(1)}, u32[]{:S(2)}, u32[]{:S(2)}) collective-permute-start(bf16[64,1024]{1,0:T(8,128)(2,1)S(1)} %collective-permute-done.25.refs_26_), channel_id=1, source_target_pairs={{0,8},{8,16},{16,24},{24,32},{32,40},{40,48},{48,56},{56,64},{64,7... | collective-permute-start | bytes 393224 | tf_op jit(solution)/shard_map/ppermute | solution.py:38
  97.8 9.1 %collective-permute-start.28 = (bf16[64,1024]{1,0:T(8,128)(2,1)S(1)}, bf16[64,1024]{1,0:T(8,128)(2,1)S(1)}, u32[]{:S(2)}, u32[]{:S(2)}) collective-permute-start(bf16[64,1024]{1,0:T(8,128)(2,1)S(1)} %collective-permute-done.14.refs_15_), channel_id=1, source_target_pairs={{0,8},{8,16},{16,24},{24,32},{32,40},{40,48},{48,56},{56,64},{64,7... | collective-permute-start | bytes 393224 | tf_op jit(solution)/shard_map/ppermute | solution.py:38
  99.4 21.2 %collective-permute-start.3 = (bf16[384,512]{1,0:T(8,128)(2,1)S(1)}, bf16[384,512]{1,0:T(8,128)(2,1)S(1)}, u32[]{:S(2)}, u32[]{:S(2)}) collective-permute-start(bf16[384,512]{1,0:T(8,128)(2,1)S(1)} %slice.4), channel_id=1, source_target_pairs={{0,2},{2,4},{4,6},{6,0},{1,3},{3,5},{5,7},{7,1},{8,10},{10,12},{12... | collective-permute-start | bytes 1179656 | tf_op jit(solution)/shard_map/ppermute | solution.py:38
  104.3 6.4 %collective-permute-start.21 = (bf16[64,1024]{1,0:T(8,128)(2,1)S(1)}, bf16[64,1024]{1,0:T(8,128)(2,1)S(1)}, u32[]{:S(2)}, u32[]{:S(2)}) collective-permute-start(bf16[64,1024]{1,0:T(8,128)(2,1)S(1)} %collective-permute-done.20.refs_21_), channel_id=1, source_target_pairs={{0,120},{8,0},{16,8},{24,16},{32,24},{40,32},{48,40},{56,48},{64,5... | collective-permute-start | bytes 393224 | tf_op jit(solution)/shard_map/ppermute | solution.py:38
  106.9 6.2 %collective-permute-start.29 = (bf16[64,1024]{1,0:T(8,128)(2,1)S(1)}, bf16[64,1024]{1,0:T(8,128)(2,1)S(1)}, u32[]{:S(2)}, u32[]{:S(2)}) collective-permute-start(bf16[64,1024]{1,0:T(8,128)(2,1)S(1)} %collective-permute-done.28.refs_9_), channel_id=1, source_target_pairs={{0,8},{8,16},{16,24},{24,32},{32,40},{40,48},{48,56},{56,64},{64,7... | collective-permute-start | bytes 393224 | tf_op jit(solution)/shard_map/ppermute | solution.py:38
  110.6 7.8 %collective-permute-start.33 = (bf16[64,1024]{1,0:T(8,128)(2,1)S(1)}, bf16[64,1024]{1,0:T(8,128)(2,1)S(1)}, u32[]{:S(2)}, u32[]{:S(2)}) collective-permute-start(bf16[64,1024]{1,0:T(8,128)(2,1)S(1)} %collective-permute-done.26.refs_27_), channel_id=1, source_target_pairs={{0,8},{8,16},{16,24},{24,32},{32,40},{40,48},{48,56},{56,64},{64,7... | collective-permute-start | bytes 393224 | tf_op jit(solution)/shard_map/ppermute | solution.py:38
  118.4 11.1 %collective-permute-start.27 = (bf16[64,1024]{1,0:T(8,128)(2,1)S(1)}, bf16[64,1024]{1,0:T(8,128)(2,1)S(1)}, u32[]{:S(2)}, u32[]{:S(2)}) collective-permute-start(bf16[64,1024]{1,0:T(8,128)(2,1)S(1)} %collective-permute-done.9.refs_10_), channel_id=1, source_target_pairs={{0,120},{8,0},{16,8},{24,16},{32,24},{40,32},{48,40},{56,48},{64,5... | collective-permute-start | bytes 393224 | tf_op jit(solution)/shard_map/ppermute | solution.py:38
  119.0 10.4 %collective-permute-start.30 = (bf16[64,1024]{1,0:T(8,128)(2,1)S(1)}, bf16[64,1024]{1,0:T(8,128)(2,1)S(1)}, u32[]{:S(2)}, u32[]{:S(2)}) collective-permute-start(bf16[64,1024]{1,0:T(8,128)(2,1)S(1)} %collective-permute-done.29.refs_8_), channel_id=1, source_target_pairs={{0,8},{8,16},{16,24},{24,32},{32,40},{40,48},{48,56},{56,64},{64,7... | collective-permute-start | bytes 393224 | tf_op jit(solution)/shard_map/ppermute | solution.py:38
  120.4 9.0 %collective-permute-start.34 = (bf16[64,1024]{1,0:T(8,128)(2,1)S(1)}, bf16[64,1024]{1,0:T(8,128)(2,1)S(1)}, u32[]{:S(2)}, u32[]{:S(2)}) collective-permute-start(bf16[64,1024]{1,0:T(8,128)(2,1)S(1)} %collective-permute-done.33.refs_13_), channel_id=1, source_target_pairs={{0,8},{8,16},{16,24},{24,32},{32,40},{40,48},{48,56},{56,64},{64,7... | collective-permute-start | bytes 393224 | tf_op jit(solution)/shard_map/ppermute | solution.py:38
  120.6 8.9 %collective-permute-start.32 = (bf16[64,1024]{1,0:T(8,128)(2,1)S(1)}, bf16[64,1024]{1,0:T(8,128)(2,1)S(1)}, u32[]{:S(2)}, u32[]{:S(2)}) collective-permute-start(bf16[64,1024]{1,0:T(8,128)(2,1)S(1)} %collective-permute-done.31.refs_10_), channel_id=1, source_target_pairs={{0,120},{8,0},{16,8},{24,16},{32,24},{40,32},{48,40},{56,48},{64,5... | collective-permute-start | bytes 393224 | tf_op jit(solution)/shard_map/ppermute | solution.py:38
  132.6 14.7 %collective-permute-start.37 = (bf16[1408,512]{1,0:T(8,128)(2,1)S(1)}, bf16[1408,512]{1,0:T(8,128)(2,1)}, u32[]{:S(2)}, u32[]{:S(2)}) collective-permute-start(bf16[1408,512]{1,0:T(8,128)(2,1)S(1)} %pack.1.refs_0_.refs_2_), channel_id=1, source_target_pairs={{0,1},{1,0},{2,3},{3,2},{4,5},{5,4},{6,7},{7,6},{8,9},{9,8},{10,11... | collective-permute-start | bytes 4325384 | tf_op jit(solution)/shard_map/ppermute | solution.py:42
  133.0 14.2 %collective-permute-start.40 = (bf16[1408,512]{1,0:T(8,128)(2,1)S(1)}, bf16[1408,512]{1,0:T(8,128)(2,1)}, u32[]{:S(2)}, u32[]{:S(2)}) collective-permute-start(bf16[1408,512]{1,0:T(8,128)(2,1)S(1)} %collective-permute-done.2.refs_3_.refs_5_), channel_id=1, source_target_pairs={{0,1},{1,0},{2,3},{3,2},{4,5},{5,4},{6,7},{7,6},{8,9},{9,8},{10,11... | collective-permute-start | bytes 4325384 | tf_op jit(solution)/shard_map/ppermute | solution.py:42
  133.2 14.1 %collective-permute-start.38 = (bf16[1408,512]{1,0:T(8,128)(2,1)}, bf16[1408,512]{1,0:T(8,128)(2,1)}, u32[]{:S(2)}, u32[]{:S(2)}) collective-permute-start(bf16[1408,512]{1,0:T(8,128)(2,1)} %collective-permute-done.1.refs_1_.refs_3_), channel_id=1, source_target_pairs={{0,1},{1,0},{2,3},{3,2},{4,5},{5,4},{6,7},{7,6},{8,9},{9,8},{10,11... | collective-permute-start | bytes 4325384 | tf_op jit(solution)/shard_map/ppermute | solution.py:42
  133.6 32.0 %collective-permute-start.39 = (bf16[1408,512]{1,0:T(8,128)(2,1)}, bf16[1408,512]{1,0:T(8,128)(2,1)}, u32[]{:S(2)}, u32[]{:S(2)}) collective-permute-start(bf16[1408,512]{1,0:T(8,128)(2,1)} %collective-permute-done.36.refs_2_), channel_id=1, source_target_pairs={{0,1},{1,0},{2,3},{3,2},{4,5},{5,4},{6,7},{7,6},{8,9},{9,8},{10,11... | collective-permute-start | bytes 4325384 | tf_op jit(solution)/shard_map/ppermute | solution.py:42
  142.1 23.5 %all-to-all-start = ((bf16[16,64,128]{2,1,0:T(8,128)(2,1)}), bf16[16,64,128]{2,1,0:T(8,128)(2,1)S(1)}, u32[]{:S(2)}, u32[]{:S(2)}) async-start(bf16[16,64,128]{2,1,0:T(8,128)(2,1)} %mixer.1), calls=%async_computation | async-start | bytes 524288 | tf_op jit(solution)/shard_map/all_to_all | solution.py:473
  (15 other events, 424.9 us)

commit v2 on v1

--- a/solution.py
+++ b/solution.py
@@ -44,13 +44,16 @@
 
 def columns_kernel(*refs):
     attn, rec = refs[0:3], refs[3:6]
-    out_ref, wide_ref, sems = refs[6:]
+    out_ref, sems = refs[6:]
     _, local, is_attn = place_of_head()
     at = pl.ds(pl.multiple_of(local * HEAD, HEAD), HEAD)
 
     def columns(sources):
         copies = [
-            pltpu.make_async_copy(sources[k].at[:, at], wide_ref.at[k], sems.at[k]) for k in range(3)
+            pltpu.make_async_copy(
+                sources[k].at[:, at], out_ref.at[:, k * HEAD : (k + 1) * HEAD], sems.at[k]
+            )
+            for k in range(3)
         ]
         for copy in copies:
             copy.start()
@@ -64,9 +67,6 @@
     @pl.when(jnp.logical_not(is_attn))
     def _():
         columns(rec)
-
-    for k in range(3):
-        out_ref[k * HEAD : (k + 1) * HEAD, :] = wide_ref[k].T
 
 
 def pack_kernel(mine_ref, other_ref, out_attn, out_rec, pack_ref, sems):
@@ -80,13 +80,16 @@
     head, _, _ = place_of_head()
     holds = holder_of(head) == lax.axis_index("tp")
 
+    used = mine_ref.shape[1]
+    pack_ref[2 * rows :, used:] = jnp.zeros((mine_ref.shape[0], pack_ref.shape[1] - used), bf16)
+
     @pl.when(holds)
     def _():
-        pack_ref[2 * rows :, :] = mine_ref[...]
+        pack_ref[2 * rows :, :used] = mine_ref[...]
 
     @pl.when(jnp.logical_not(holds))
     def _():
-        pack_ref[2 * rows :, :] = other_ref[...]
+        pack_ref[2 * rows :, :used] = other_ref[...]
 
     for copy in copies:
         copy.wait()
@@ -103,7 +106,7 @@
     count = (len(refs) - 3) // 2
     near, far = refs[:count], refs[count : 2 * count]
     rows, half = near[0].shape
-    each = packs[0].shape[1]
+    each = near[0].shape[1] * 2 // fs
     x, t = lax.axis_index("fs"), lax.axis_index("tp")
     _, local, _ = place_of_head()
     at_a = pl.ds(pl.multiple_of(t * half, half), half)
@@ -123,14 +126,15 @@
         return 0
 
     lax.fori_loop(0, count, normalize, 0)
-    group = 4 * rows
+    group = 2 * rows
 
     def multiply(k, _):
         own = pl.ds(pl.multiple_of(k * group, group), group)
         product = 0.0
         for step in range(fs):
             at = pl.ds(pl.multiple_of((x + step) % fs * each, each), each)
-            product += mm_t(norm_ref[own, at], packs[step][packs[step].shape[0] - 3 * HEAD :, :])
+            weight = packs[step][packs[step].shape[0] - each :, 0 : 3 * HEAD]
+            product += mm(norm_ref[own, at], weight)
         product = product.astype(bf16)
         to = pl.ds(pl.multiple_of(done + k * group, group), group)
         query_ref[to, :] = product[:, :HEAD]
@@ -377,14 +381,13 @@
     far = swap(lax.dynamic_slice_in_dim(own, (1 - t) * rows, rows, 0))
 
     depth, wide = out_attn.shape
-    shape = jax.ShapeDtypeStruct((3 * HEAD, attn_query.shape[0]), bf16)
+    shape = jax.ShapeDtypeStruct((attn_query.shape[0], 3 * HEAD), bf16)
     pick = pl.pallas_call(
         columns_kernel,
         out_shape=shape,
         in_specs=[outside] * 6,
         out_specs=whole,
         scratch_shapes=[
-            pltpu.VMEM((3, attn_query.shape[0], HEAD), bf16),
             pltpu.SemaphoreType.DMA((3,)),
         ],
         compiler_params=limit(6),
@@ -403,7 +406,7 @@
     )
     pack = pack(*resident([columns, columns_other]), *left_out([out_attn, out_rec]))
     from_prev, from_next = shift(pack, "fs", 1), shift(pack, "fs", -1)
-    far_columns = from_prev[2 * depth :]
+    far_columns = from_prev[2 * depth :, : 3 * HEAD]
     far_columns = shift(far_columns, "fs", 1)
     from_far = shift(from_prev, "fs", 1)
     mine = [pack, from_next, from_far, from_prev]

time: 172 us -> 183 us (1.064)
  the two profiles are of different devices: /device:TPU:40 before, /device:TPU:42 now
where the time goes in v2:
time: 183 us
  waiting for transfers between devices  105 us (57%)
  starting transfers between devices  52.1 us (28%)
  Pallas kernels  24.6 us (13%)
    ppermute x34, waiting for transfers between devices, shift(): return lax.ppermute(x, axis, ring(lax.axis_size(axis), step))  83.4 us
    ppermute x34, starting transfers between devices, shift(): return lax.ppermute(x, axis, ring(lax.axis_size(axis), step))  46.6 us
    all_to_all x1, waiting for transfers between devices, body(): lax.all_to_all(mixed_heads, 'sp', split_axis=0, concat_axis=0, tiled=True)  18.2 us
    pallas_call x2, Pallas kernels, project(): pl.pallas_call(functools.partial(project_kernel, done), out_shape=(jax.Sh...  9.37 us
    pallas_call x1, Pallas kernels, body(): pl.pallas_call(mixer_kernel, out_shape=jax.ShapeDtypeStruct((sp, rows, HE...  6.94 us
    pallas_call x1, Pallas kernels, body(): pl.pallas_call(output_kernel, out_shape=jax.ShapeDtypeStruct((rows, fs *...  6 us
    all_to_all x1, starting transfers between devices, body(): lax.all_to_all(mixed_heads, 'sp', split_axis=0, concat_axis=0, tiled=True)  3.97 us
  transfers between devices with their start and end apart: 42, of which 30 were waited for; matrix products, arithmetic and copies ran while one was open for 0% of the time, Pallas kernels for 9%

profile of v2, /device:TPU:42, one launch (start us, length us, event | category | flops | bytes accessed | tf_op | source)
XLA Modules:
  0.0 182.8 jit_solution(13673410212027577034)
XLA Ops:
  1.3 1.7 collective-permute-done.other_ref
  4.2 1.7 collective-permute-start.2
  6.3 34.4 %collective-permute-done.2.refs_3_.refs_5_ = bf16[1536,512]{1,0:T(8,128)(2,1)S(1)} collective-permute-done((bf16[1536,512]{1,0:T(8,128)(2,1)S(1)}, bf16[1536,512]{1,0:T(8,128)(2,1)S(1)}, u32[]{:S(2)}, u32[]{:S(2)}) %collective-permute-start.2) | collective-permute-done | bytes 1572896 | tf_op jit(solution)/shard_map/ppermute | solution.py:38
  40.7 1.6 collective-permute-start.36
  42.5 22.5 %collective-permute-start.4 = (bf16[64,1024]{1,0:T(8,128)(2,1)S(1)}, bf16[64,1024]{1,0:T(8,128)(2,1)S(1)}, u32[]{:S(2)}, u32[]{:S(2)}) collective-permute-start(bf16[64,1024]{1,0:T(8,128)(2,1)S(1)} %get-tuple-element.14.refs_4_), channel_id=1, source_target_pairs={{0,120},{8,0},{16,8},{24,16},{32,24},{40,32},{48,40},{56,48},{64,5... | collective-permute-start | bytes 393224 | tf_op jit(solution)/shard_map/ppermute | solution.py:38
  65.0 3.2 %collective-permute-start.16 = (bf16[64,1024]{1,0:T(8,128)(2,1)S(1)}, bf16[64,1024]{1,0:T(8,128)(2,1)S(1)}, u32[]{:S(2)}, u32[]{:S(2)}) collective-permute-start(bf16[64,1024]{1,0:T(8,128)(2,1)S(1)} %collective-permute-done.15.refs_16_), channel_id=1, source_target_pairs={{0,120},{8,0},{16,8},{24,16},{32,24},{40,32},{48,40},{56,48},{64,5... | collective-permute-start | bytes 393224 | tf_op jit(solution)/shard_map/ppermute | solution.py:38
  68.4 3.7 %collective-permute-start.5 = (bf16[64,1024]{1,0:T(8,128)(2,1)S(1)}, bf16[64,1024]{1,0:T(8,128)(2,1)S(1)}, u32[]{:S(2)}, u32[]{:S(2)}) collective-permute-start(bf16[64,1024]{1,0:T(8,128)(2,1)S(1)} %collective-permute-done.4.refs_5_), channel_id=1, source_target_pairs={{0,120},{8,0},{16,8},{24,16},{32,24},{40,32},{48,40},{56,48},{64,5... | collective-permute-start | bytes 393224 | tf_op jit(solution)/shard_map/ppermute | solution.py:38
  72.3 2.4 %collective-permute-done.5.refs_6_ = bf16[64,1024]{1,0:T(8,128)(2,1)S(1)} collective-permute-done((bf16[64,1024]{1,0:T(8,128)(2,1)S(1)}, bf16[64,1024]{1,0:T(8,128)(2,1)S(1)}, u32[]{:S(2)}, u32[]{:S(2)}) %collective-permute-start.5) | collective-permute-done | bytes 131104 | tf_op jit(solution)/shard_map/ppermute | solution.py:38
  74.7 3.7 %collective-permute-start.17 = (bf16[64,1024]{1,0:T(8,128)(2,1)S(1)}, bf16[64,1024]{1,0:T(8,128)(2,1)S(1)}, u32[]{:S(2)}, u32[]{:S(2)}) collective-permute-start(bf16[64,1024]{1,0:T(8,128)(2,1)S(1)} %collective-permute-done.16.refs_17_), channel_id=1, source_target_pairs={{0,120},{8,0},{16,8},{24,16},{32,24},{40,32},{48,40},{56,48},{64,5... | collective-permute-start | bytes 393224 | tf_op jit(solution)/shard_map/ppermute | solution.py:38
  81.4 3.6 %collective-permute-done.6.refs_7_ = bf16[64,1024]{1,0:T(8,128)(2,1)S(1)} collective-permute-done((bf16[64,1024]{1,0:T(8,128)(2,1)S(1)}, bf16[64,1024]{1,0:T(8,128)(2,1)S(1)}, u32[]{:S(2)}, u32[]{:S(2)}) %collective-permute-start.6) | collective-permute-done | bytes 131104 | tf_op jit(solution)/shard_map/ppermute | solution.py:38
  90.0 3.2 %collective-permute-done.7.refs_8_ = bf16[64,1024]{1,0:T(8,128)(2,1)S(1)} collective-permute-done((bf16[64,1024]{1,0:T(8,128)(2,1)S(1)}, bf16[64,1024]{1,0:T(8,128)(2,1)S(1)}, u32[]{:S(2)}, u32[]{:S(2)}) %collective-permute-start.7) | collective-permute-done | bytes 131104 | tf_op jit(solution)/shard_map/ppermute | solution.py:38
  94.5 1.8 collective-permute-done.13.refs_14_
  96.6 2.2 %collective-permute-done.19.refs_20_ = bf16[64,1024]{1,0:T(8,128)(2,1)S(1)} collective-permute-done((bf16[64,1024]{1,0:T(8,128)(2,1)S(1)}, bf16[64,1024]{1,0:T(8,128)(2,1)S(1)}, u32[]{:S(2)}, u32[]{:S(2)}) %collective-permute-start.19) | collective-permute-done | bytes 131104 | tf_op jit(solution)/shard_map/ppermute | solution.py:38
  99.6 2.0 %collective-permute-done.8.refs_9_ = bf16[64,1024]{1,0:T(8,128)(2,1)S(1)} collective-permute-done((bf16[64,1024]{1,0:T(8,128)(2,1)S(1)}, bf16[64,1024]{1,0:T(8,128)(2,1)S(1)}, u32[]{:S(2)}, u32[]{:S(2)}) %collective-permute-start.8) | collective-permute-done | bytes 131104 | tf_op jit(solution)/shard_map/ppermute | solution.py:38
  102.5 2.0 %collective-permute-start.9 = (bf16[64,1024]{1,0:T(8,128)(2,1)S(1)}, bf16[64,1024]{1,0:T(8,128)(2,1)S(1)}, u32[]{:S(2)}, u32[]{:S(2)}) collective-permute-start(bf16[64,1024]{1,0:T(8,128)(2,1)S(1)} %collective-permute-done.8.refs_9_), channel_id=1, source_target_pairs={{0,120},{8,0},{16,8},{24,16},{32,24},{40,32},{48,40},{56,48},{64,5... | collective-permute-start | bytes 393224 | tf_op jit(solution)/shard_map/ppermute | solution.py:38
  104.6 1.8 collective-permute-done.14.refs_15_
  106.3 1.5 collective-permute-done.20.refs_21_
  109.3 1.8 %collective-permute-start.21 = (bf16[64,1024]{1,0:T(8,128)(2,1)S(1)}, bf16[64,1024]{1,0:T(8,128)(2,1)S(1)}, u32[]{:S(2)}, u32[]{:S(2)}) collective-permute-start(bf16[64,1024]{1,0:T(8,128)(2,1)S(1)} %collective-permute-done.20.refs_21_), channel_id=1, source_target_pairs={{0,120},{8,0},{16,8},{24,16},{32,24},{40,32},{48,40},{56,48},{64,5... | collective-permute-start | bytes 393224 | tf_op jit(solution)/shard_map/ppermute | solution.py:38
  111.1 2.2 %collective-permute-done.28.refs_9_ = bf16[64,1024]{1,0:T(8,128)(2,1)S(1)} collective-permute-done((bf16[64,1024]{1,0:T(8,128)(2,1)S(1)}, bf16[64,1024]{1,0:T(8,128)(2,1)S(1)}, u32[]{:S(2)}, u32[]{:S(2)}) %collective-permute-start.28) | collective-permute-done | bytes 131104 | tf_op jit(solution)/shard_map/ppermute | solution.py:38
  116.4 4.1 %collective-permute-done.29.refs_8_ = bf16[64,1024]{1,0:T(8,128)(2,1)S(1)} collective-permute-done((bf16[64,1024]{1,0:T(8,128)(2,1)S(1)}, bf16[64,1024]{1,0:T(8,128)(2,1)S(1)}, u32[]{:S(2)}, u32[]{:S(2)}) %collective-permute-start.29) | collective-permute-done | bytes 131104 | tf_op jit(solution)/shard_map/ppermute | solution.py:38
  120.5 2.8 %collective-permute-done.33.refs_13_ = bf16[64,1024]{1,0:T(8,128)(2,1)S(1)} collective-permute-done((bf16[64,1024]{1,0:T(8,128)(2,1)S(1)}, bf16[64,1024]{1,0:T(8,128)(2,1)S(1)}, u32[]{:S(2)}, u32[]{:S(2)}) %collective-permute-start.33) | collective-permute-done | bytes 131104 | tf_op jit(solution)/shard_map/ppermute | solution.py:38
  123.3 3.3 %collective-permute-done.27.refs_6_ = bf16[64,1024]{1,0:T(8,128)(2,1)S(1)} collective-permute-done((bf16[64,1024]{1,0:T(8,128)(2,1)S(1)}, bf16[64,1024]{1,0:T(8,128)(2,1)S(1)}, u32[]{:S(2)}, u32[]{:S(2)}) %collective-permute-start.27) | collective-permute-done | bytes 131104 | tf_op jit(solution)/shard_map/ppermute | solution.py:38
  126.7 1.6 collective-permute-done.31.refs_10_
  128.3 4.5 %collective-permute-done.30.refs_7_ = bf16[64,1024]{1,0:T(8,128)(2,1)S(1)} collective-permute-done((bf16[64,1024]{1,0:T(8,128)(2,1)S(1)}, bf16[64,1024]{1,0:T(8,128)(2,1)S(1)}, u32[]{:S(2)}, u32[]{:S(2)}) %collective-permute-start.30) | collective-permute-done | bytes 131104 | tf_op jit(solution)/shard_map/ppermute | solution.py:38
  132.8 1.6 collective-permute-done.34.refs_12_
  135.5 6.3 %project.2 = (bf16[768,128]{1,0:T(8,128)(2,1)S(1)}, bf16[768,256]{1,0:T(8,128)(2,1)S(1)}) custom-call(f32[1,2048]{1,0:T(1,128)S(1)} %bitcast.7, f32[4]{0:T(128)S(1)} %copy-done.3, f32[4,128]{1,0:T(4,128)S(1)} %copy-done.2, bf16[1536,512]{1,0:T(8,128)(2,1)S(1)} %pack.1.refs_0_.refs_2_, bf16[1536,512]{1,0:T(8,128)(2,1)} %collective-permute-done.1.refs_1_.refs_3_, ...), custom_call_target="tpu_custom_call" | custom-call | tf_op jit(solution)/shard_map/project/pallas_call | solution.py:433
  141.8 3.1 %project.3 = (bf16[1024,128]{1,0:T(8,128)(2,1)S(1)}, bf16[1040,256]{1,0:T(8,128)(2,1)S(1)}) custom-call(f32[1,2048]{1,0:T(1,128)S(1)} %bitcast.8, f32[4]{0:T(128)S(1)} %copy-done.3, f32[4,128]{1,0:T(4,128)S(1)} %copy-done.2, bf16[768,128]{1,0:T(8,128)(2,1)S(1)} %get-tuple-element.9.refs_0_, bf16[768,256]{1,0:T(8,128)(2,1)S(1)} %get-tuple-element.10.refs_1_, ...), custom_call_target="tpu_custom_call" | custom-call | tf_op jit(solution)/shard_map/project/pallas_call | solution.py:433
  145.2 1.8 collective-permute-done.35.other_ref
  147.0 6.9 %mixer.1 = bf16[16,64,128]{2,1,0:T(8,128)(2,1)S(1)} custom-call(f32[1,128]{1,0:T(1,128)S(1)} %bitcast.9, bf16[1024,128]{1,0:T(8,128)(2,1)S(1)} %get-tuple-element.11.query_ref, bf16[1040,256]{1,0:T(8,128)(2,1)S(1)} %get-tuple-element.12.mine_ref, bf16[1040,256]{1,0:T(8,128)(2,1)S(1)} %collective-permute-done.35.other_ref), custom_call_target="tpu_custom_call" | custom-call | tf_op jit(solution)/shard_map/mixer/pallas_call | solution.py:459
  154.6 4.0 %all-to-all-start = ((bf16[16,64,128]{2,1,0:T(8,128)(2,1)}), bf16[16,64,128]{2,1,0:T(8,128)(2,1)S(1)}, u32[]{:S(2)}, u32[]{:S(2)}) async-start(bf16[16,64,128]{2,1,0:T(8,128)(2,1)} %copy-done), calls=%async_computation | async-start | bytes 524288 | tf_op jit(solution)/shard_map/all_to_all | solution.py:476
  158.6 18.2 %all-to-all-done.heads_ref = bf16[16,64,128]{2,1,0:T(8,128)(2,1)S(1)} async-done(((bf16[16,64,128]{2,1,0:T(8,128)(2,1)}), bf16[16,64,128]{2,1,0:T(8,128)(2,1)S(1)}, u32[]{:S(2)}, u32[]{:S(2)}) %all-to-all-start) | async-done | bytes 262176 | tf_op jit(solution)/shard_map/all_to_all | solution.py:476
  176.8 6.0 %output.1 = bf16[64,2048]{1,0:T(8,128)(2,1)} custom-call(bf16[16,64,128]{2,1,0:T(8,128)(2,1)S(1)} %all-to-all-done.heads_ref, bf16[1536,512]{1,0:T(8,128)(2,1)S(1)} %pack.1.refs_0_.refs_2_, bf16[1536,512]{1,0:T(8,128)(2,1)} %collective-permute-done.1.refs_1_.refs_3_, bf16[1536,512]{1,0:T(8,128)(2,1)} %collective-permute-done.36.refs_2_, ...), custom_call_target="tpu_custom_call" | custom-call | tf_op jit(solution)/shard_map/output/pallas_call | solution.py:477
  (72 shorter events, 21.3 us)
Async XLA Ops:
  4.2 36.5 %collective-permute-start.2 = (bf16[1536,512]{1,0:T(8,128)(2,1)S(1)}, bf16[1536,512]{1,0:T(8,128)(2,1)S(1)}, u32[]{:S(2)}, u32[]{:S(2)}) collective-permute-start(bf16[1536,512]{1,0:T(8,128)(2,1)S(1)} %pack.1.refs_0_.refs_2_), channel_id=1, source_target_pairs={{0,2},{2,4},{4,6},{6,0},{1,3},{3,5},{5,7},{7,1},{8,10},{10,12},{12... | collective-permute-start | bytes 4718600 | tf_op jit(solution)/shard_map/ppermute | solution.py:38
  5.9 128.6 %collective-permute-start.1 = (bf16[1536,512]{1,0:T(8,128)(2,1)S(1)}, bf16[1536,512]{1,0:T(8,128)(2,1)}, u32[]{:S(2)}, u32[]{:S(2)}) collective-permute-start(bf16[1536,512]{1,0:T(8,128)(2,1)S(1)} %pack.1.refs_0_.refs_2_), channel_id=1, source_target_pairs={{0,6},{2,0},{4,2},{6,4},{1,7},{3,1},{5,3},{7,5},{8,14},{10,8},{12,... | collective-permute-start | bytes 4718600 | tf_op jit(solution)/shard_map/ppermute | solution.py:38
  40.7 94.4 %collective-permute-start.36 = (bf16[1536,512]{1,0:T(8,128)(2,1)S(1)}, bf16[1536,512]{1,0:T(8,128)(2,1)}, u32[]{:S(2)}, u32[]{:S(2)}) collective-permute-start(bf16[1536,512]{1,0:T(8,128)(2,1)S(1)} %collective-permute-done.2.refs_3_.refs_5_), channel_id=1, source_target_pairs={{0,2},{2,4},{4,6},{6,0},{1,3},{3,5},{5,7},{7,1},{8,10},{10,12},{12... | collective-permute-start | bytes 4718600 | tf_op jit(solution)/shard_map/ppermute | solution.py:38
  42.4 22.6 %collective-permute-start.15 = (bf16[64,1024]{1,0:T(8,128)(2,1)S(1)}, bf16[64,1024]{1,0:T(8,128)(2,1)S(1)}, u32[]{:S(2)}, u32[]{:S(2)}) collective-permute-start(bf16[64,1024]{1,0:T(8,128)(2,1)S(1)} %get-tuple-element.13), channel_id=1, source_target_pairs={{0,1},{1,0},{2,3},{3,2},{4,5},{5,4},{6,7},{7,6},{8,9},{9,8},{10,11... | collective-permute-start | bytes 393224 | tf_op jit(solution)/shard_map/ppermute | solution.py:42
  42.5 25.9 %collective-permute-start.4 = (bf16[64,1024]{1,0:T(8,128)(2,1)S(1)}, bf16[64,1024]{1,0:T(8,128)(2,1)S(1)}, u32[]{:S(2)}, u32[]{:S(2)}) collective-permute-start(bf16[64,1024]{1,0:T(8,128)(2,1)S(1)} %get-tuple-element.14.refs_4_), channel_id=1, source_target_pairs={{0,120},{8,0},{16,8},{24,16},{32,24},{40,32},{48,40},{56,48},{64,5... | collective-permute-start | bytes 393224 | tf_op jit(solution)/shard_map/ppermute | solution.py:38
  65.0 7.1 %collective-permute-start.10 = (bf16[64,1024]{1,0:T(8,128)(2,1)S(1)}, bf16[64,1024]{1,0:T(8,128)(2,1)S(1)}, u32[]{:S(2)}, u32[]{:S(2)}) collective-permute-start(bf16[64,1024]{1,0:T(8,128)(2,1)S(1)} %get-tuple-element.14.refs_4_), channel_id=1, source_target_pairs={{0,8},{8,16},{16,24},{24,32},{32,40},{40,48},{48,56},{56,64},{64,7... | collective-permute-start | bytes 393224 | tf_op jit(solution)/shard_map/ppermute | solution.py:38
  65.0 7.1 %collective-permute-start.16 = (bf16[64,1024]{1,0:T(8,128)(2,1)S(1)}, bf16[64,1024]{1,0:T(8,128)(2,1)S(1)}, u32[]{:S(2)}, u32[]{:S(2)}) collective-permute-start(bf16[64,1024]{1,0:T(8,128)(2,1)S(1)} %collective-permute-done.15.refs_16_), channel_id=1, source_target_pairs={{0,120},{8,0},{16,8},{24,16},{32,24},{40,32},{48,40},{56,48},{64,5... | collective-permute-start | bytes 393224 | tf_op jit(solution)/shard_map/ppermute | solution.py:38
  68.4 6.2 %collective-permute-start.5 = (bf16[64,1024]{1,0:T(8,128)(2,1)S(1)}, bf16[64,1024]{1,0:T(8,128)(2,1)S(1)}, u32[]{:S(2)}, u32[]{:S(2)}) collective-permute-start(bf16[64,1024]{1,0:T(8,128)(2,1)S(1)} %collective-permute-done.4.refs_5_), channel_id=1, source_target_pairs={{0,120},{8,0},{16,8},{24,16},{32,24},{40,32},{48,40},{56,48},{64,5... | collective-permute-start | bytes 393224 | tf_op jit(solution)/shard_map/ppermute | solution.py:38
  72.1 7.1 %collective-permute-start.22 = (bf16[64,1024]{1,0:T(8,128)(2,1)S(1)}, bf16[64,1024]{1,0:T(8,128)(2,1)S(1)}, u32[]{:S(2)}, u32[]{:S(2)}) collective-permute-start(bf16[64,1024]{1,0:T(8,128)(2,1)S(1)} %collective-permute-done.15.refs_16_), channel_id=1, source_target_pairs={{0,8},{8,16},{16,24},{24,32},{32,40},{40,48},{48,56},{56,64},{64,7... | collective-permute-start | bytes 393224 | tf_op jit(solution)/shard_map/ppermute | solution.py:38
  72.2 8.5 %collective-permute-start.11 = (bf16[64,1024]{1,0:T(8,128)(2,1)S(1)}, bf16[64,1024]{1,0:T(8,128)(2,1)S(1)}, u32[]{:S(2)}, u32[]{:S(2)}) collective-permute-start(bf16[64,1024]{1,0:T(8,128)(2,1)S(1)} %collective-permute-done.10.refs_11_), channel_id=1, source_target_pairs={{0,8},{8,16},{16,24},{24,32},{32,40},{40,48},{48,56},{56,64},{64,7... | collective-permute-start | bytes 393224 | tf_op jit(solution)/shard_map/ppermute | solution.py:38
  74.7 6.6 %collective-permute-start.17 = (bf16[64,1024]{1,0:T(8,128)(2,1)S(1)}, bf16[64,1024]{1,0:T(8,128)(2,1)S(1)}, u32[]{:S(2)}, u32[]{:S(2)}) collective-permute-start(bf16[64,1024]{1,0:T(8,128)(2,1)S(1)} %collective-permute-done.16.refs_17_), channel_id=1, source_target_pairs={{0,120},{8,0},{16,8},{24,16},{32,24},{40,32},{48,40},{56,48},{64,5... | collective-permute-start | bytes 393224 | tf_op jit(solution)/shard_map/ppermute | solution.py:38
  80.7 6.3 %collective-permute-start.23 = (bf16[64,1024]{1,0:T(8,128)(2,1)S(1)}, bf16[64,1024]{1,0:T(8,128)(2,1)S(1)}, u32[]{:S(2)}, u32[]{:S(2)}) collective-permute-start(bf16[64,1024]{1,0:T(8,128)(2,1)S(1)} %collective-permute-done.22.refs_23_), channel_id=1, source_target_pairs={{0,8},{8,16},{16,24},{24,32},{32,40},{40,48},{48,56},{56,64},{64,7... | collective-permute-start | bytes 393224 | tf_op jit(solution)/shard_map/ppermute | solution.py:38
  81.3 7.0 %collective-permute-start.12 = (bf16[64,1024]{1,0:T(8,128)(2,1)S(1)}, bf16[64,1024]{1,0:T(8,128)(2,1)S(1)}, u32[]{:S(2)}, u32[]{:S(2)}) collective-permute-start(bf16[64,1024]{1,0:T(8,128)(2,1)S(1)} %collective-permute-done.11.refs_12_), channel_id=1, source_target_pairs={{0,8},{8,16},{16,24},{24,32},{32,40},{40,48},{48,56},{56,64},{64,7... | collective-permute-start | bytes 393224 | tf_op jit(solution)/shard_map/ppermute | solution.py:38
  86.9 6.2 %collective-permute-start.7 = (bf16[64,1024]{1,0:T(8,128)(2,1)S(1)}, bf16[64,1024]{1,0:T(8,128)(2,1)S(1)}, u32[]{:S(2)}, u32[]{:S(2)}) collective-permute-start(bf16[64,1024]{1,0:T(8,128)(2,1)S(1)} %collective-permute-done.6.refs_7_), channel_id=1, source_target_pairs={{0,120},{8,0},{16,8},{24,16},{32,24},{40,32},{48,40},{56,48},{64,5... | collective-permute-start | bytes 393224 | tf_op jit(solution)/shard_map/ppermute | solution.py:38
  88.3 6.2 %collective-permute-start.24 = (bf16[64,1024]{1,0:T(8,128)(2,1)S(1)}, bf16[64,1024]{1,0:T(8,128)(2,1)S(1)}, u32[]{:S(2)}, u32[]{:S(2)}) collective-permute-start(bf16[64,1024]{1,0:T(8,128)(2,1)S(1)} %collective-permute-done.23.refs_24_), channel_id=1, source_target_pairs={{0,8},{8,16},{16,24},{24,32},{32,40},{40,48},{48,56},{56,64},{64,7... | collective-permute-start | bytes 393224 | tf_op jit(solution)/shard_map/ppermute | solution.py:38
  90.0 6.4 %collective-permute-start.13 = (bf16[64,1024]{1,0:T(8,128)(2,1)S(1)}, bf16[64,1024]{1,0:T(8,128)(2,1)S(1)}, u32[]{:S(2)}, u32[]{:S(2)}) collective-permute-start(bf16[64,1024]{1,0:T(8,128)(2,1)S(1)} %collective-permute-done.12.refs_13_), channel_id=1, source_target_pairs={{0,8},{8,16},{16,24},{24,32},{32,40},{40,48},{48,56},{56,64},{64,7... | collective-permute-start | bytes 393224 | tf_op jit(solution)/shard_map/ppermute | solution.py:38
  94.5 7.0 %collective-permute-start.8 = (bf16[64,1024]{1,0:T(8,128)(2,1)S(1)}, bf16[64,1024]{1,0:T(8,128)(2,1)S(1)}, u32[]{:S(2)}, u32[]{:S(2)}) collective-permute-start(bf16[64,1024]{1,0:T(8,128)(2,1)S(1)} %collective-permute-done.7.refs_8_), channel_id=1, source_target_pairs={{0,120},{8,0},{16,8},{24,16},{32,24},{40,32},{48,40},{56,48},{64,5... | collective-permute-start | bytes 393224 | tf_op jit(solution)/shard_map/ppermute | solution.py:38
  96.4 6.2 %collective-permute-start.25 = (bf16[64,1024]{1,0:T(8,128)(2,1)S(1)}, bf16[64,1024]{1,0:T(8,128)(2,1)S(1)}, u32[]{:S(2)}, u32[]{:S(2)}) collective-permute-start(bf16[64,1024]{1,0:T(8,128)(2,1)S(1)} %collective-permute-done.24.refs_25_), channel_id=1, source_target_pairs={{0,8},{8,16},{16,24},{24,32},{32,40},{40,48},{48,56},{56,64},{64,7... | collective-permute-start | bytes 393224 | tf_op jit(solution)/shard_map/ppermute | solution.py:38
  98.8 7.6 %collective-permute-start.14 = (bf16[64,1024]{1,0:T(8,128)(2,1)S(1)}, bf16[64,1024]{1,0:T(8,128)(2,1)S(1)}, u32[]{:S(2)}, u32[]{:S(2)}) collective-permute-start(bf16[64,1024]{1,0:T(8,128)(2,1)S(1)} %collective-permute-done.13.refs_14_), channel_id=1, source_target_pairs={{0,8},{8,16},{16,24},{24,32},{32,40},{40,48},{48,56},{56,64},{64,7... | collective-permute-start | bytes 393224 | tf_op jit(solution)/shard_map/ppermute | solution.py:38
  101.6 6.3 %collective-permute-start.20 = (bf16[64,1024]{1,0:T(8,128)(2,1)S(1)}, bf16[64,1024]{1,0:T(8,128)(2,1)S(1)}, u32[]{:S(2)}, u32[]{:S(2)}) collective-permute-start(bf16[64,1024]{1,0:T(8,128)(2,1)S(1)} %collective-permute-done.19.refs_20_), channel_id=1, source_target_pairs={{0,120},{8,0},{16,8},{24,16},{32,24},{40,32},{48,40},{56,48},{64,5... | collective-permute-start | bytes 393224 | tf_op jit(solution)/shard_map/ppermute | solution.py:38
  102.5 6.7 %collective-permute-start.9 = (bf16[64,1024]{1,0:T(8,128)(2,1)S(1)}, bf16[64,1024]{1,0:T(8,128)(2,1)S(1)}, u32[]{:S(2)}, u32[]{:S(2)}) collective-permute-start(bf16[64,1024]{1,0:T(8,128)(2,1)S(1)} %collective-permute-done.8.refs_9_), channel_id=1, source_target_pairs={{0,120},{8,0},{16,8},{24,16},{32,24},{40,32},{48,40},{56,48},{64,5... | collective-permute-start | bytes 393224 | tf_op jit(solution)/shard_map/ppermute | solution.py:38
  106.3 6.9 %collective-permute-start.28 = (bf16[64,1024]{1,0:T(8,128)(2,1)S(1)}, bf16[64,1024]{1,0:T(8,128)(2,1)S(1)}, u32[]{:S(2)}, u32[]{:S(2)}) collective-permute-start(bf16[64,1024]{1,0:T(8,128)(2,1)S(1)} %collective-permute-done.14.refs_15_), channel_id=1, source_target_pairs={{0,8},{8,16},{16,24},{24,32},{32,40},{40,48},{48,56},{56,64},{64,7... | collective-permute-start | bytes 393224 | tf_op jit(solution)/shard_map/ppermute | solution.py:38
  107.9 6.8 %collective-permute-start.26 = (bf16[64,1024]{1,0:T(8,128)(2,1)S(1)}, bf16[64,1024]{1,0:T(8,128)(2,1)S(1)}, u32[]{:S(2)}, u32[]{:S(2)}) collective-permute-start(bf16[64,1024]{1,0:T(8,128)(2,1)S(1)} %collective-permute-done.25.refs_26_), channel_id=1, source_target_pairs={{0,8},{8,16},{16,24},{24,32},{32,40},{40,48},{48,56},{56,64},{64,7... | collective-permute-start | bytes 393224 | tf_op jit(solution)/shard_map/ppermute | solution.py:38
  113.2 7.3 %collective-permute-start.29 = (bf16[64,1024]{1,0:T(8,128)(2,1)S(1)}, bf16[64,1024]{1,0:T(8,128)(2,1)S(1)}, u32[]{:S(2)}, u32[]{:S(2)}) collective-permute-start(bf16[64,1024]{1,0:T(8,128)(2,1)S(1)} %collective-permute-done.28.refs_9_), channel_id=1, source_target_pairs={{0,8},{8,16},{16,24},{24,32},{32,40},{40,48},{48,56},{56,64},{64,7... | collective-permute-start | bytes 393224 | tf_op jit(solution)/shard_map/ppermute | solution.py:38
  114.7 8.7 %collective-permute-start.33 = (bf16[64,1024]{1,0:T(8,128)(2,1)S(1)}, bf16[64,1024]{1,0:T(8,128)(2,1)S(1)}, u32[]{:S(2)}, u32[]{:S(2)}) collective-permute-start(bf16[64,1024]{1,0:T(8,128)(2,1)S(1)} %collective-permute-done.26.refs_27_), channel_id=1, source_target_pairs={{0,8},{8,16},{16,24},{24,32},{32,40},{40,48},{48,56},{56,64},{64,7... | collective-permute-start | bytes 393224 | tf_op jit(solution)/shard_map/ppermute | solution.py:38
  115.0 20.0 %collective-permute-start.3 = (bf16[512,384]{1,0:T(8,128)(2,1)S(1)}, bf16[512,384]{1,0:T(8,128)(2,1)S(1)}, u32[]{:S(2)}, u32[]{:S(2)}) collective-permute-start(bf16[512,384]{1,0:T(8,128)(2,1)S(1)} %slice.4), channel_id=1, source_target_pairs={{0,2},{2,4},{4,6},{6,0},{1,3},{3,5},{5,7},{7,1},{8,10},{10,12},{12... | collective-permute-start | bytes 1179656 | tf_op jit(solution)/shard_map/ppermute | solution.py:38
  132.8 9.0 %collective-permute-start.32 = (bf16[64,1024]{1,0:T(8,128)(2,1)S(1)}, bf16[64,1024]{1,0:T(8,128)(2,1)S(1)}, u32[]{:S(2)}, u32[]{:S(2)}) collective-permute-start(bf16[64,1024]{1,0:T(8,128)(2,1)S(1)} %collective-permute-done.31.refs_10_), channel_id=1, source_target_pairs={{0,120},{8,0},{16,8},{24,16},{32,24},{40,32},{48,40},{56,48},{64,5... | collective-permute-start | bytes 393224 | tf_op jit(solution)/shard_map/ppermute | solution.py:38
  134.5 24.1 %collective-permute-start.37 = (bf16[1536,512]{1,0:T(8,128)(2,1)S(1)}, bf16[1536,512]{1,0:T(8,128)(2,1)}, u32[]{:S(2)}, u32[]{:S(2)}) collective-permute-start(bf16[1536,512]{1,0:T(8,128)(2,1)S(1)} %pack.1.refs_0_.refs_2_), channel_id=1, source_target_pairs={{0,1},{1,0},{2,3},{3,2},{4,5},{5,4},{6,7},{7,6},{8,9},{9,8},{10,11... | collective-permute-start | bytes 4718600 | tf_op jit(solution)/shard_map/ppermute | solution.py:42
  134.5 24.1 %collective-permute-start.40 = (bf16[1536,512]{1,0:T(8,128)(2,1)S(1)}, bf16[1536,512]{1,0:T(8,128)(2,1)}, u32[]{:S(2)}, u32[]{:S(2)}) collective-permute-start(bf16[1536,512]{1,0:T(8,128)(2,1)S(1)} %collective-permute-done.2.refs_3_.refs_5_), channel_id=1, source_target_pairs={{0,1},{1,0},{2,3},{3,2},{4,5},{5,4},{6,7},{7,6},{8,9},{9,8},{10,11... | collective-permute-start | bytes 4718600 | tf_op jit(solution)/shard_map/ppermute | solution.py:42
  135.0 23.6 %collective-permute-start.38 = (bf16[1536,512]{1,0:T(8,128)(2,1)}, bf16[1536,512]{1,0:T(8,128)(2,1)}, u32[]{:S(2)}, u32[]{:S(2)}) collective-permute-start(bf16[1536,512]{1,0:T(8,128)(2,1)} %collective-permute-done.1.refs_1_.refs_3_), channel_id=1, source_target_pairs={{0,1},{1,0},{2,3},{3,2},{4,5},{5,4},{6,7},{7,6},{8,9},{9,8},{10,11... | collective-permute-start | bytes 4718600 | tf_op jit(solution)/shard_map/ppermute | solution.py:42
  135.1 41.7 %collective-permute-start.39 = (bf16[1536,512]{1,0:T(8,128)(2,1)}, bf16[1536,512]{1,0:T(8,128)(2,1)}, u32[]{:S(2)}, u32[]{:S(2)}) collective-permute-start(bf16[1536,512]{1,0:T(8,128)(2,1)} %collective-permute-done.36.refs_2_), channel_id=1, source_target_pairs={{0,1},{1,0},{2,3},{3,2},{4,5},{5,4},{6,7},{7,6},{8,9},{9,8},{10,11... | collective-permute-start | bytes 4718600 | tf_op jit(solution)/shard_map/ppermute | solution.py:42
  154.6 22.2 %all-to-all-start = ((bf16[16,64,128]{2,1,0:T(8,128)(2,1)}), bf16[16,64,128]{2,1,0:T(8,128)(2,1)S(1)}, u32[]{:S(2)}, u32[]{:S(2)}) async-start(bf16[16,64,128]{2,1,0:T(8,128)(2,1)} %copy-done), calls=%async_computation | async-start | bytes 524288 | tf_op jit(solution)/shard_map/all_to_all | solution.py:476
  (16 other events, 499.9 us)
